TPU v7x, 256 devices: a whole 4x4x8 slice. The times are simulated.
256 devices in a mesh: kv: 64 (over z, y, core), tp: 4 (over x).
Axes of the slice: x: 4, y: 4, z: 8, core: 2. Of those that a mesh axis runs over, the one named last changes fastest.
Arguments:
- tokens: bfloat16 [512, 6, 4096], P('kv'), may hold values from -6 to 6
- norm_gain: float32 [4096], replicated, may hold values from 0.1 to 1.9
- w_query: bfloat16 [4096, 2048], P('kv', 'tp'), may hold values from -0.09375 to 0.09375
- w_key: bfloat16 [4096, 2048], P('kv', 'tp'), may hold values from -0.09375 to 0.09375
- w_value: bfloat16 [4096, 2048], P('kv', 'tp'), may hold values from -0.09375 to 0.09375
- w_outgate: bfloat16 [4096, 2048], P('kv', 'tp'), may hold values from -0.09375 to 0.09375
- w_gates: bfloat16 [4096, 2, 16], P('kv', None, 'tp'), may hold values from -0.09375 to 0.09375
- forget_bias: float32 [16], P('tp'), may hold values from 1 to 6
- head_gain: float32 [2048], P('tp'), may hold values from 0.1 to 1.9
- w_mix: bfloat16 [2048, 4096], P('tp', 'kv'), may hold values from -0.125 to 0.125
- state_cell: float32 [512, 16, 128, 128], P('kv', 'tp'), may hold values from -4 to 4
- state_norm: float32 [512, 16, 128], P('kv', 'tp'), may hold values from -4 to 4
- state_max: float32 [512, 16], P('kv', 'tp'), may hold values from -4 to 120
- pend_keys: bfloat16 [512, 6, 2048], P('kv', None, 'tp'), may hold values from -6 to 6
- pend_values: bfloat16 [512, 6, 2048], P('kv', None, 'tp'), may hold values from -6 to 6
- pend_gates: float32 [512, 6, 2, 16], P('kv', None, None, 'tp'), may hold values from -6 to 6
- accepted: int32 [512], P('kv'), may hold values from 0 to 6
Outputs:
- mixed: bfloat16 [512, 6, 4096], P('kv', None, 'tp')
- new_cell: float32 [512, 16, 128, 128], P('kv', 'tp')
- new_norm: float32 [512, 16, 128], P('kv', 'tp')
- new_max: float32 [512, 16], P('kv', 'tp')
All inputs are finite; a program needn't handle non-finite values.
Results may differ from a plain program's by a relative error of at most 0.018.
Values may be sent and summed in bfloat16 or wider, within the bound.
No kernel may reach another device: no remote copies, remote signals or barrier semaphores. Data moves between devices by JAX's collectives and lax.ppermute only.
A program may use at most 128 MiB of HBM per device.

v0:
```python
import jax
import jax.numpy as jnp
from jax import lax
from jax.sharding import PartitionSpec as P

epsilon = 1e-06
very_low = -1e30
highest = lax.Precision.HIGHEST


def sent_together(arrays, axis, dim, along):
    columns = [a.reshape(*a.shape[:along], -1) for a in arrays]
    both = jnp.concatenate(columns, axis=along)
    whole, at, outs = (lax.all_gather(both, axis, axis=dim, tiled=True), 0, [])
    for a, column in zip(arrays, columns):
        slab = whole[..., at : at + column.shape[along]]
        outs.append(slab.reshape(*slab.shape[:along], *a.shape[along:]))
        at += column.shape[along]
    return tuple(outs)


def in_blocks(shard, dim, peers):
    before, after = (shard.shape[:dim], shard.shape[dim + 1 :])
    return jnp.moveaxis(shard.reshape(*before, peers, -1, *after), dim, 0)


def summed_on_arrival(shard, axis, dim):
    parts = in_blocks(shard, dim, lax.axis_size(axis))
    arrived = lax.all_to_all(parts, axis, split_axis=0, concat_axis=0, tiled=True)
    return arrived.astype(jnp.float32).sum(axis=0)


def fold_pending(
    cell_state, normer, stabilizer, key_rows, value_rows, gate_rows, forget_shift, accepted
):
    proposals = key_rows.shape[1]
    accepted_mask = jnp.arange(proposals)[None, :, None] < accepted[:, None, None]
    log_in = jnp.where(accepted_mask, gate_rows[:, :, 0, :], very_low)
    log_keep = jnp.where(
        accepted_mask, jax.nn.log_sigmoid(gate_rows[:, :, 1, :] + forget_shift), 0.0
    )
    running = jnp.cumsum(log_keep, axis=1)
    block_total = running[:, -1]
    log_w = block_total[:, None, :] - running + log_in
    new_max = jnp.maximum(block_total + stabilizer, jnp.max(log_w, axis=1))
    weights = jnp.exp(log_w - new_max[:, None, :])
    carried = jnp.exp(block_total + stabilizer - new_max)
    weighted_keys = weights[..., None] * key_rows
    cell_new = carried[..., None, None] * cell_state + jnp.einsum(
        "sphd,sphe->shde", weighted_keys, value_rows, precision=highest
    )
    norm_new = carried[..., None] * normer + jnp.sum(weighted_keys, axis=1)
    return (cell_new, norm_new, new_max)


def read_block(queries, key_rows, value_rows, log_in, log_keep, cell_state, normer, stabilizer):
    proposals = queries.shape[1]
    causal = jnp.arange(proposals)[:, None] >= jnp.arange(proposals)[None, :]
    running_h = jnp.moveaxis(jnp.cumsum(log_keep, axis=1), 1, 2)
    input_h = jnp.moveaxis(log_in, 1, 2)
    log_d = jnp.where(
        causal, running_h[..., :, None] - running_h[..., None, :] + input_h[..., None, :], very_low
    )
    log_p = running_h + stabilizer[..., None]
    top_log = jnp.maximum(log_p, jnp.max(log_d, axis=-1))
    decays = jnp.exp(log_d - top_log[..., None])
    prior_w = jnp.exp(log_p - top_log)
    scores = jnp.einsum("sthd,suhd->shtu", queries, key_rows, precision=highest) * decays
    numerator = jnp.einsum("shtu,suhe->shte", scores, value_rows, precision=highest)
    numerator = numerator + prior_w[..., None] * jnp.einsum(
        "sthd,shde->shte", queries, cell_state, precision=highest
    )
    denominator = jnp.sum(scores, axis=-1) + prior_w * jnp.einsum(
        "sthd,shd->sht", queries, normer, precision=highest
    )
    hidden_out = numerator / jnp.maximum(jnp.abs(denominator), jnp.exp(-top_log))[..., None]
    return jnp.moveaxis(hidden_out, 1, 2)


def shards(
    tokens,
    norm_gain,
    w_query,
    w_key,
    w_value,
    w_outgate,
    w_gates,
    forget_bias,
    head_gain,
    w_mix,
    state_cell,
    state_norm,
    state_max,
    pend_keys,
    pend_values,
    pend_gates,
    accepted,
):
    sequences, proposals, model_width = tokens.shape
    token_count = sequences * proposals
    local_heads = forget_bias.shape[0]
    head_size = state_cell.shape[-1]
    flat_rows = tokens.reshape(token_count, model_width)
    widened = flat_rows.astype(jnp.float32)
    sum_squares = jnp.sum(widened * widened, axis=-1)
    scaled_in = (widened * norm_gain).astype(jnp.bfloat16)
    pieces = sent_together((w_query, w_key, w_value, w_outgate, w_gates), "kv", 0, 1)
    totals = tuple(
        (
            jnp.dot(
                scaled_in,
                shard_piece.reshape(shard_piece.shape[0], -1),
                preferred_element_type=jnp.float32,
            )
            for shard_piece in pieces
        )
    )
    row_scale = lax.rsqrt(sum_squares / model_width + epsilon)[:, None]
    queries = (totals[0] * row_scale).astype(jnp.bfloat16)
    new_keys = (totals[1] * row_scale).astype(jnp.bfloat16)
    new_values = (totals[2] * row_scale).astype(jnp.bfloat16)
    outgate = (totals[3] * row_scale).astype(jnp.bfloat16)
    gate_pre = (totals[4] * row_scale).reshape(sequences, proposals, 2, local_heads)

    def split_heads(array):
        return array.astype(jnp.float32).reshape(sequences, proposals, local_heads, head_size)

    key_scale = head_size ** (-0.5)
    cell_new, norm_new, new_max = fold_pending(
        state_cell,
        state_norm,
        state_max,
        split_heads(pend_keys) * key_scale,
        split_heads(pend_values),
        pend_gates,
        forget_bias,
        accepted,
    )
    log_in = gate_pre[:, :, 0, :]
    log_keep = jax.nn.log_sigmoid(gate_pre[:, :, 1, :] + forget_bias)
    hidden = read_block(
        split_heads(queries),
        split_heads(new_keys) * key_scale,
        split_heads(new_values),
        log_in,
        log_keep,
        cell_new,
        norm_new,
        new_max,
    )
    normed = hidden * lax.rsqrt(jnp.mean(hidden * hidden, axis=-1, keepdims=True) + epsilon)
    normed = normed * head_gain.reshape(local_heads, head_size)
    gated_rows = (jax.nn.sigmoid(split_heads(outgate)) * normed).astype(jnp.bfloat16)
    gated_rows = gated_rows.reshape(token_count, local_heads * head_size)
    partial_out = jnp.dot(
        gated_rows,
        lax.all_gather(w_mix, "kv", axis=1, tiled=True),
        preferred_element_type=jnp.float32,
    )
    mixed_out = summed_on_arrival(partial_out.astype(jnp.bfloat16), "tp", 1).astype(jnp.bfloat16)
    return (mixed_out.reshape(sequences, proposals, -1), cell_new, norm_new, new_max)


def solution(mesh):
    return jax.shard_map(
        shards,
        mesh=mesh,
        in_specs=(
            P("kv", None, None),
            P(),
            P("kv", "tp"),
            P("kv", "tp"),
            P("kv", "tp"),
            P("kv", "tp"),
            P("kv", None, "tp"),
            P("tp"),
            P("tp"),
            P("tp", "kv"),
            P("kv", "tp", None, None),
            P("kv", "tp", None),
            P("kv", "tp"),
            P("kv", None, "tp"),
            P("kv", None, "tp"),
            P("kv", None, None, "tp"),
            P("kv"),
        ),
        out_specs=(
            P("kv", None, "tp"),
            P("kv", "tp", None, None),
            P("kv", "tp", None),
            P("kv", "tp"),
        ),
        check_vma=False,
    )
```

profile of v0, /device:TPU:1, one launch (start us, length us, event | category | flops | bytes accessed | tf_op | source)
XLA Modules:
  0.0 221.1 jit_solution(15016051348541972806)
XLA Ops:
  7.3 1.0 constant_dynamic-update-slice_fusion.4
  8.3 0.8 copy.116
  9.0 0.8 constant_dynamic-update-slice_fusion.3
  9.9 0.8 constant_dynamic-update-slice_fusion.2
  10.7 0.8 constant_dynamic-update-slice_fusion.1
  11.6 0.7 copy-done.3
  12.4 0.7 all-gather.5.cloned.1.call-update
  13.1 1.2 copy.115
  14.4 0.2 multiply_reduce_fusion
  15.3 103.3 %all-gather.3.cloned.1.call-done = bf16[4096,2056]{1,0:T(8,128)(2,1)} async-done(((bf16[64,2056]{1,0:T(8,128)(2,1)}), bf16[4096,2056]{1,0:T(8,128)(2,1)}) %all-gather.3.cloned.1.call-update) | async-done | bytes 16842768 | tf_op jit(solution)/shard_map/all_gather | solution.py:14
  118.5 1.6 convolution_multiply_fusion.1
  120.3 0.1 fusion.70
  120.4 1.4 reduce_window_sum.18
  122.1 0.2 fusion.79
  122.6 3.0 %fusion.35 = bf16[48,512]{1,0:T(8,128)(2,1)S(1)} fusion(bf16[48,4096]{1,0:T(8,128)(2,1)S(1)} %multiply_convert_fusion, bf16[4096,2056]{1,0:T(8,128)(2,1)} %all-gather.3.cloned.1.call-done, f32[48]{0:T(128)S(1)} %rsqrt.19), kind=kOutput, calls=%fused_computation.24 | convolution fusion | flops 201375744 | bytes 4636864 | tf_op jit(solution)/shard_map/dot_general | solution.py:110
  125.7 1.4 reduce_window_sum.17
  127.1 3.0 %fusion.32 = f32[48,512]{1,0:T(8,128)S(1)} fusion(bf16[48,4096]{1,0:T(8,128)(2,1)S(1)} %multiply_convert_fusion, bf16[4096,2056]{1,0:T(8,128)(2,1)} %all-gather.3.cloned.1.call-done, f32[48]{0:T(128)S(1)} %rsqrt.19), kind=kOutput, calls=%fused_computation.23 | convolution fusion | flops 201424896 | bytes 4686016 | tf_op jit(solution)/shard_map/dot_general | solution.py:110
  130.1 3.2 %fusion.23 = bf16[48,512]{1,0:T(8,128)(2,1)S(1)} fusion(bf16[48,4096]{1,0:T(8,128)(2,1)S(1)} %multiply_convert_fusion, bf16[4096,2056]{1,0:T(8,128)(2,1)} %all-gather.3.cloned.1.call-done, f32[48]{0:T(128)S(1)} %rsqrt.19), kind=kOutput, calls=%fused_computation.20 | convolution fusion | flops 201375744 | bytes 4636864 | tf_op jit(solution)/shard_map/dot_general | solution.py:110
  133.3 3.0 %fusion.53 = f32[48,512]{1,0:T(8,128)S(1)} fusion(bf16[48,4096]{1,0:T(8,128)(2,1)S(1)} %multiply_convert_fusion, bf16[4096,2056]{1,0:T(8,128)(2,1)} %all-gather.3.cloned.1.call-done, f32[48]{0:T(128)S(1)} %rsqrt.19), kind=kOutput, calls=%fused_computation.31 | convolution fusion | flops 201474048 | bytes 4686016 | tf_op jit(solution)/shard_map/dot_general | solution.py:110
  136.4 0.2 fusion.59
  136.7 0.2 fusion.62
  137.0 0.3 fusion.82
  137.4 3.7 %multiply_add_fusion = f32[8,4,128,128]{3,2,1,0:T(8,128)S(1)} fusion(f32[8,4,128,128]{3,2,1,0:T(8,128)} %param.27, f32[8,4]{1,0:T(8,128)S(1)} %get-tuple-element.20, f32[8,6,4,128]{3,0,2,1:T(8,128)S(1)} %convert_bitcast_fusion, bf16[8,6,4,128]{3,0,2,1:T(8,128)(2,1)S(1)} %bitcast.90, f32[8,6,4]{1,2,0:T(4,128)S(1)} %exponential_multiply_fusion), kind=kOutput, calls=%fused_computation.9 | convolution fusion | flops 38821888 | bytes 4342656 | tf_op jit(solution)/shard_map/sphd,sphe->shde/dot_general | solution.py:49
  141.1 1.1 fusion.10
  142.2 0.4 multiply_reduce_fusion.1
  142.8 54.7 %all-gather.5.cloned.1.call-done = bf16[512,4096]{0,1:T(8,128)(2,1)} async-done(((bf16[512,64]{0,1:T(8,128)(2,1)}), bf16[512,4096]{0,1:T(8,128)(2,1)}) %all-gather.5.cloned.1.call-update) | async-done | bytes 4194320 | tf_op jit(solution)/shard_map/all_gather | solution.py:157
  197.5 3.5 %convolution_convert_fusion = bf16[48,4096]{1,0:T(8,128)(2,1)S(1)} fusion(bf16[512,4096]{0,1:T(8,128)(2,1)} %all-gather.5.cloned.1.call-done, bf16[6,8,4,128]{3,2,1,0:T(4,128)(2,1)S(1)} %bitcast.94), kind=kOutput, calls=%fused_computation | convolution fusion | flops 201523200 | bytes 4636672 | tf_op jit(solution)/shard_map/dot_general | solution.py:155
  201.1 0.8 copy.183
  201.8 4.0 %all-to-all-start = ((bf16[4,48,1024]{2,1,0:T(8,128)(2,1)}), bf16[4,48,1024]{2,1,0:T(8,128)(2,1)S(1)}, u32[]{:S(2)}, u32[]{:S(2)}) async-start(bf16[4,48,1024]{2,1,0:T(8,128)(2,1)} %bitcast.89), calls=%async_computation | async-start | bytes 786432 | tf_op jit(solution)/shard_map/all_to_all | solution.py:29
  205.8 0.7 copy.138
  206.5 7.0 %all-to-all-done = bf16[4,48,1024]{2,1,0:T(8,128)(2,1)S(1)} async-done(((bf16[4,48,1024]{2,1,0:T(8,128)(2,1)}), bf16[4,48,1024]{2,1,0:T(8,128)(2,1)S(1)}, u32[]{:S(2)}, u32[]{:S(2)}) %all-to-all-start) | async-done | bytes 393248 | tf_op jit(solution)/shard_map/all_to_all | solution.py:29
  213.5 0.7 copy.137
  (64 shorter events, 2.2 us)
Async XLA Ops:
  7.2 130.2 %copy-start = (bf16[8,6,512]{2,0,1:T(8,128)(2,1)S(1)}, bf16[8,6,512]{2,0,1:T(8,128)(2,1)}, u32[]{:S(2)}) copy-start(bf16[8,6,512]{2,0,1:T(8,128)(2,1)} %param.31) | copy-start | bytes 147460
  7.2 7.3 %copy-start.2 = (bf16[8,6,4096]{2,0,1:T(8,128)(2,1)S(1)}, bf16[8,6,4096]{2,0,1:T(8,128)(2,1)}, u32[]{:S(2)}) copy-start(bf16[8,6,4096]{2,0,1:T(8,128)(2,1)} %param.17) | copy-start | bytes 1179652
  7.2 7.6 %copy-start.5 = (f32[8,6,2,4]{0,3,2,1:T(4,128)S(1)}, f32[8,6,2,4]{0,3,2,1:T(4,128)}, u32[]{:S(2)}) copy-start(f32[8,6,2,4]{0,3,2,1:T(4,128)} %param.32) | copy-start | bytes 4612
  7.2 7.8 %copy-start.10 = (f32[8,4]{0,1:T(4,128)S(1)}, f32[8,4]{0,1:T(4,128)}, u32[]{:S(2)}) copy-start(f32[8,4]{0,1:T(4,128)} %param.29) | copy-start | bytes 388
  7.2 7.9 %copy-start.12 = (s32[8]{0:T(128)S(1)}, s32[8]{0:T(128)}, u32[]{:S(2)}) copy-start(s32[8]{0:T(128)} %param.33) | copy-start | bytes 100
  7.2 8.0 %copy-start.4 = (bf16[8,6,512]{2,0,1:T(8,128)(2,1)S(1)}, bf16[8,6,512]{2,0,1:T(8,128)(2,1)}, u32[]{:S(2)}) copy-start(bf16[8,6,512]{2,0,1:T(8,128)(2,1)} %param.30) | copy-start | bytes 147460
  7.2 8.0 %copy-start.6 = (f32[4096]{0:T(1024)S(1)}, f32[4096]{0:T(1024)}, u32[]{:S(2)}) copy-start(f32[4096]{0:T(1024)} %param.18) | copy-start | bytes 49156
  7.2 113.0 %copy-start.11 = (f32[4]{0:T(128)S(1)}, f32[4]{0:T(128)}, u32[]{:S(2)}) copy-start(f32[4]{0:T(128)} %param.24) | copy-start | bytes 52
  7.3 111.3 %all-gather.3.cloned.1.call-start = ((), (), s32[]{:S(2)}) async-start(), calls=%async_computation.1 | async-start | bytes 18104320 | tf_op jit(solution)/shard_map/all_gather | solution.py:14
  11.6 0.7 copy-start.3
  12.3 185.2 %all-gather.5.cloned.1.call-start = ((), (), s32[]{:S(2)}) async-start(), calls=%async_computation.2 | async-start | bytes 4259840 | tf_op jit(solution)/shard_map/all_gather | solution.py:157
  130.1 6.5 %copy-start.7 = (f32[8,4,128]{2,1,0:T(4,128)S(1)}, f32[8,4,128]{2,1,0:T(4,128)}, u32[]{:S(2)}) copy-start(f32[8,4,128]{2,1,0:T(4,128)} %param.28) | copy-start | bytes 49156
  136.7 5.9 %copy-start.8 = (f32[8,4,128]{2,1,0:T(4,128)}, f32[8,4,128]{2,1,0:T(4,128)S(1)}, u32[]{:S(2)}) copy-start(f32[8,4,128]{2,1,0:T(4,128)S(1)} %multiply_add_fusion.1) | copy-start | bytes 49156
  137.0 5.7 %copy-start.9 = (f32[512]{0:T(512)S(1)}, f32[512]{0:T(512)}, u32[]{:S(2)}) copy-start(f32[512]{0:T(512)} %param.25) | copy-start | bytes 6148
  141.1 60.7 %copy-start.1 = (f32[8,4,128,128]{3,2,1,0:T(8,128)}, f32[8,4,128,128]{3,2,1,0:T(8,128)S(1)}, u32[]{:S(2)}) copy-start(f32[8,4,128,128]{3,2,1,0:T(8,128)S(1)} %multiply_add_fusion) | copy-start | bytes 6291460
  201.8 11.6 %all-to-all-start = ((bf16[4,48,1024]{2,1,0:T(8,128)(2,1)}), bf16[4,48,1024]{2,1,0:T(8,128)(2,1)S(1)}, u32[]{:S(2)}, u32[]{:S(2)}) async-start(bf16[4,48,1024]{2,1,0:T(8,128)(2,1)} %bitcast.89), calls=%async_computation | async-start | bytes 786432 | tf_op jit(solution)/shard_map/all_to_all | solution.py:29
Sparse Core Ops, SparseCore 0:
  12.4 106.0 all-gather.2
  121.3 76.1 all-gather.4
where the time goes:
time: 222 us; the launch traced here: 221 us
  waiting for transfers between devices  166 us (75%)
  matrix products  23.1 us (10%)
  between operations  14.4 us (6%)
  local copies, waits for them, and re-layouts  9.62 us (4%)
  other arithmetic  4.21 us (2%)
  starting transfers between devices  4.06 us (2%)
    all_gather x1, waiting for transfers between devices, sent_together(): whole, at, outs = (lax.all_gather(both, axis, axis=dim, tiled=True), 0, [])  103 us
    all_gather x1, waiting for transfers between devices, shards(): lax.all_gather(w_mix, 'kv', axis=1, tiled=True)  54.7 us
    dot_general x5, matrix products, shards(): jnp.dot(scaled_in, shard_piece.reshape(shard_piece.shape[0], -1), preferr...  13.9 us
    all_to_all x1, waiting for transfers between devices, summed_on_arrival(): lax.all_to_all(parts, axis, split_axis=0, concat_axis=0, tiled=True)  6.96 us
    unnamed x36, local copies, waits for them, and re-layouts  6.01 us
  transfers between devices with their start and end apart: 3, of which 3 were waited for; matrix products, arithmetic and copies ran while one was open for 12% of the time, Pallas kernels for 0%

commit v1 on v0

v1 whole, which is shorter than its diff:
```python
import functools

import jax
import jax.numpy as jnp
from jax import lax
from jax.experimental import pallas as pl
from jax.experimental.pallas import tpu as pltpu
from jax.sharding import Mesh
from jax.sharding import PartitionSpec as P

epsilon = 1e-06
very_low = -1e30
highest = lax.Precision.HIGHEST
bf16 = jnp.bfloat16
f32 = jnp.float32
in_vmem = pl.BlockSpec(memory_space=pltpu.VMEM)
in_smem = pl.BlockSpec(memory_space=pltpu.SMEM)


def shift(array, axis, by):
    n = lax.axis_size(axis)
    return lax.ppermute(array, axis, [(j, (j + by) % n) for j in range(n)])


def ring(chunk, axis):
    n = lax.axis_size(axis)
    chunks = [chunk] + [None] * (n - 1)
    ahead = behind = chunk
    for s in range(1, n // 2 + 1):
        ahead = shift(ahead, axis, 1)
        chunks[s] = ahead
        if n - s > s:
            behind = shift(behind, axis, -1)
            chunks[n - s] = behind
    return chunks


def direct(chunk, axis):
    return [chunk] + [shift(chunk, axis, s) for s in range(1, lax.axis_size(axis))]


def call(kernel, out_shape, *args, flops=0, scratch=()):
    outs = jax.tree.leaves(out_shape)
    nbytes = sum(a.size * a.dtype.itemsize for a in (*args, *outs))
    return pl.pallas_call(
        kernel,
        out_shape=out_shape,
        in_specs=[in_smem if a.dtype == jnp.int32 else in_vmem for a in args],
        out_specs=jax.tree.map(lambda _: in_vmem, out_shape),
        scratch_shapes=list(scratch),
        compiler_params=pltpu.CompilerParams(vmem_limit_bytes=32 * 2**20),
        cost_estimate=pl.CostEstimate(flops=max(flops, 2 * nbytes), bytes_accessed=nbytes, transcendentals=0),
    )(*args)


def pack_kernel(*refs):
    *ins, out = refs
    at = 0
    for ref in ins:
        width = ref.shape[1]
        out[:, at : at + width] = ref[...]
        at += width


def prep_kernel(nz, ny, place, tokens, gain, out, squares):
    z, y, c = place[0], place[1], place[2]
    rows, width = tokens.shape
    unit = width // (nz * ny)
    wide = tokens[...].astype(f32)
    squares[...] = jnp.sum(wide * wide, axis=-1, keepdims=True)
    for sz in range(nz):
        for sy in range(ny):
            block = lax.rem(z - sz + nz, nz) * ny + lax.rem(y + sy, ny)
            lanes = pl.ds(pl.multiple_of(block * unit, unit), unit)
            scaled = tokens[:, lanes].astype(f32) * gain[:, lanes]
            scaled = jnp.where(c == 1, pltpu.roll(scaled, unit // 2, 1), scaled)
            out[sy, :, sz * unit : (sz + 1) * unit] = scaled.astype(bf16)


def project_kernel(n, groups, gates, *refs):
    xs, mine, other, out = refs[:groups], refs[groups : groups + n], refs[groups + n : groups + 2 * n], refs[-1]
    rows = xs[0].shape[0]
    x = jnp.concatenate([ref[...] for ref in xs], axis=0)
    total = mine[0].shape[1]
    wide = total - gates
    step = wide // 4
    for at, width in [(i * step, step) for i in range(4)] + [(wide, gates)]:
        w = jnp.concatenate([ref[:, at : at + width] for pair in zip(mine, other) for ref in pair], axis=0)
        part = jnp.dot(x, w, preferred_element_type=f32)
        high = part.astype(bf16)
        for g in range(groups):
            out[g, :, at : at + width] = high[g * rows : (g + 1) * rows]
        if width == gates:
            low = (part - high.astype(f32)).astype(bf16)
            for g in range(groups):
                out[g, :, total : total + gates] = low[g * rows : (g + 1) * rows]


def mix_kernel(n, ny, groups, *refs):
    place, gated, mine, other = refs[0], refs[1 : 1 + groups], refs[1 + groups : 1 + groups + n], refs[1 + groups + n : 1 + groups + 2 * n]
    out, held, acc = refs[-3], refs[-2], refs[-1]
    z, y, c, t = place[0], place[1], place[2], place[3]
    for g in range(groups):
        held[g] = gated[g][...]
    halves, rows, width = acc.shape
    acc[...] = jnp.zeros_like(acc)
    part_k = mine[0].shape[0]
    for s in range(n):
        owner = lax.rem(z - s + n, n)
        group = lax.rem(owner, groups)
        half = owner // groups
        from_here = lax.rem(t - group + groups, groups)
        w = jnp.concatenate([mine[s][...], other[s][...]], axis=0)
        left = held[from_here, :, :part_k]
        right = held[from_here, :, part_k:]
        g = jnp.concatenate([jnp.where(c == 0, left, right), jnp.where(c == 0, right, left)], axis=1)
        part = jnp.dot(g, w, preferred_element_type=f32).astype(bf16).astype(f32)
        acc[half] = acc[half] + part
    unit = width // ny
    for h in range(halves):
        for sy in range(ny):
            block = lax.rem(y - sy + ny, ny)
            lanes = pl.ds(pl.multiple_of(h * width + block * unit, unit), unit)
            out[:, lanes] = acc[h, :, sy * unit : (sy + 1) * unit].astype(bf16)


def fold_pending(
    cell_state, normer, stabilizer, key_rows, value_rows, gate_rows, forget_shift, accepted
):
    proposals = key_rows.shape[1]
    accepted_mask = jnp.arange(proposals)[None, :, None] < accepted[:, None, None]
    log_in = jnp.where(accepted_mask, gate_rows[:, :, 0, :], very_low)
    log_keep = jnp.where(
        accepted_mask, jax.nn.log_sigmoid(gate_rows[:, :, 1, :] + forget_shift), 0.0
    )
    running = jnp.cumsum(log_keep, axis=1)
    block_total = running[:, -1]
    log_w = block_total[:, None, :] - running + log_in
    new_max = jnp.maximum(block_total + stabilizer, jnp.max(log_w, axis=1))
    weights = jnp.exp(log_w - new_max[:, None, :])
    carried = jnp.exp(block_total + stabilizer - new_max)
    weighted_keys = weights[..., None] * key_rows
    cell_new = carried[..., None, None] * cell_state + jnp.einsum(
        "sphd,sphe->shde", weighted_keys, value_rows, precision=highest
    )
    norm_new = carried[..., None] * normer + jnp.sum(weighted_keys, axis=1)
    return (cell_new, norm_new, new_max)


def read_block(queries, key_rows, value_rows, log_in, log_keep, cell_state, normer, stabilizer):
    proposals = queries.shape[1]
    causal = jnp.arange(proposals)[:, None] >= jnp.arange(proposals)[None, :]
    running_h = jnp.moveaxis(jnp.cumsum(log_keep, axis=1), 1, 2)
    input_h = jnp.moveaxis(log_in, 1, 2)
    log_d = jnp.where(
        causal, running_h[..., :, None] - running_h[..., None, :] + input_h[..., None, :], very_low
    )
    log_p = running_h + stabilizer[..., None]
    top_log = jnp.maximum(log_p, jnp.max(log_d, axis=-1))
    decays = jnp.exp(log_d - top_log[..., None])
    prior_w = jnp.exp(log_p - top_log)
    scores = jnp.einsum("sthd,suhd->shtu", queries, key_rows, precision=highest) * decays
    numerator = jnp.einsum("shtu,suhe->shte", scores, value_rows, precision=highest)
    numerator = numerator + prior_w[..., None] * jnp.einsum(
        "sthd,shde->shte", queries, cell_state, precision=highest
    )
    denominator = jnp.sum(scores, axis=-1) + prior_w * jnp.einsum(
        "sthd,shd->sht", queries, normer, precision=highest
    )
    hidden_out = numerator / jnp.maximum(jnp.abs(denominator), jnp.exp(-top_log))[..., None]
    return jnp.moveaxis(hidden_out, 1, 2)


def shards(
    tokens, norm_gain, w_query, w_key, w_value, w_outgate, w_gates, forget_bias, head_gain, w_mix,
    state_cell, state_norm, state_max, pend_keys, pend_values, pend_gates, accepted,
):
    sequences, proposals, model_width = tokens.shape
    rows = sequences * proposals
    local_heads = forget_bias.shape[0]
    head_size = state_cell.shape[-1]
    width = local_heads * head_size
    gates = 2 * local_heads
    nz, ny, groups = lax.axis_size("z"), lax.axis_size("y"), lax.axis_size("tp")
    z, y, c, t = (lax.axis_index(a) for a in ("z", "y", "c", "tp"))
    place = jnp.stack([z, y, c, t]).astype(jnp.int32)

    depth = w_query.shape[0]
    packed = call(
        pack_kernel, jax.ShapeDtypeStruct((depth, 4 * width + gates), bf16),
        w_query, w_key, w_value, w_outgate, w_gates.reshape(depth, gates),
    )
    mine = ring(packed, "z")
    other = [shift(chunk, "c", 1) for chunk in mine]

    scaled, squares = call(
        functools.partial(prep_kernel, nz, ny),
        (jax.ShapeDtypeStruct((ny, rows, model_width // ny), bf16), jax.ShapeDtypeStruct((rows, 1), f32)),
        place, tokens.reshape(rows, model_width), norm_gain[None],
    )
    xs = [scaled[0]] + [shift(scaled[s], "y", s) for s in range(1, ny)]

    half_k = width // 2
    kept = lax.dynamic_slice_in_dim(w_mix, c * half_k, half_k, 0)
    given = shift(lax.dynamic_slice_in_dim(w_mix, (1 - c) * half_k, half_k, 0), "c", 1)
    block = jnp.where(c == 0, jnp.concatenate([kept, given], 1), jnp.concatenate([given, kept], 1))
    per = nz // groups
    moves = [(i * groups + j, ((i % per) * groups + j) * groups + i // per) for i in range(nz) for j in range(groups)]
    block = lax.ppermute(block, ("z", "tp"), moves)
    mix_mine = ring(jnp.concatenate(direct(block, "y"), axis=1), "z")
    mix_other = [shift(chunk, "c", 1) for chunk in mix_mine]

    parts = call(
        functools.partial(project_kernel, nz, ny, gates),
        jax.ShapeDtypeStruct((ny, rows, 4 * width + 2 * gates), bf16),
        *xs, *mine, *other, flops=2 * ny * rows * nz * 2 * depth * 4 * width,
    )
    home = [parts[0]] + [shift(parts[s], "y", -s) for s in range(1, ny)]
    total = functools.reduce(jnp.add, [part.astype(f32) for part in home])
    row_scale = lax.rsqrt(squares / model_width + epsilon)
    total = total * row_scale
    queries, new_keys, new_values, outgate = (total[:, i * width : (i + 1) * width].astype(bf16) for i in range(4))
    gate_pre = total[:, 4 * width : 4 * width + gates] + total[:, 4 * width + gates :]
    gate_pre = gate_pre.reshape(sequences, proposals, 2, local_heads)

    def split_heads(array):
        return array.astype(f32).reshape(sequences, proposals, local_heads, head_size)

    key_scale = head_size ** (-0.5)
    cell_new, norm_new, new_max = fold_pending(
        state_cell, state_norm, state_max, split_heads(pend_keys) * key_scale, split_heads(pend_values),
        pend_gates, forget_bias, accepted,
    )
    log_in = gate_pre[:, :, 0, :]
    log_keep = jax.nn.log_sigmoid(gate_pre[:, :, 1, :] + forget_bias)
    hidden = read_block(
        split_heads(queries), split_heads(new_keys) * key_scale, split_heads(new_values),
        log_in, log_keep, cell_new, norm_new, new_max,
    )
    normed = hidden * lax.rsqrt(jnp.mean(hidden * hidden, axis=-1, keepdims=True) + epsilon)
    normed = normed * head_gain.reshape(local_heads, head_size)
    gated = (jax.nn.sigmoid(split_heads(outgate)) * normed).astype(bf16).reshape(rows, width)

    columns = per * ny * mix_mine[0].shape[1] // ny
    mixed = call(
        functools.partial(mix_kernel, nz, ny, groups),
        jax.ShapeDtypeStruct((rows, columns), bf16),
        place, *direct(gated, "tp"), *mix_mine, *mix_other, flops=2 * rows * groups * width * columns,
        scratch=(pltpu.VMEM((groups, rows, width), bf16), pltpu.VMEM((per, rows, columns // per), f32)),
    )
    return (mixed.reshape(sequences, proposals, -1), cell_new, norm_new, new_max)


def solution(mesh):
    grid = Mesh(mesh.devices.reshape(8, 4, 2, mesh.shape["tp"]), ("z", "y", "c", "tp"))
    kv = ("z", "y", "c")
    return jax.shard_map(
        shards,
        mesh=grid,
        in_specs=(
            P(kv, None, None), P(), P(kv, "tp"), P(kv, "tp"), P(kv, "tp"), P(kv, "tp"), P(kv, None, "tp"),
            P("tp"), P("tp"), P("tp", kv), P(kv, "tp", None, None), P(kv, "tp", None), P(kv, "tp"),
            P(kv, None, "tp"), P(kv, None, "tp"), P(kv, None, None, "tp"), P(kv),
        ),
        out_specs=(P(kv, None, "tp"), P(kv, "tp", None, None), P(kv, "tp", None), P(kv, "tp")),
        check_vma=False,
    )
```

time: 222 us -> 125 us (0.56)
  waiting for transfers between devices: 166 us -> 18.6 us
  starting transfers between devices: 4.06 us -> 69.9 us
  matrix products: 23.1 us -> 5.73 us
  between operations: 14.4 us -> 1.17 us
  local copies, waits for them, and re-layouts: 9.62 us -> 16.9 us
  Pallas kernels: 0 us -> 5.39 us
    all_gather x2 -> x0, waiting for transfers between devices: 158 us -> none  [the longest x1 103 us: sent_together(): whole, at, outs = (lax.all_gather(both, axis, axis=dim, tiled=True), 0, [])]
    ppermute x0 -> x44, starting transfers between devices: none -> 69.9 us  [the longest x43 69.2 us: shift(): return lax.ppermute(array, axis, [(j, (j + by) % n) for j in range(n)])]
    ppermute x0 -> x44, waiting for transfers between devices: none -> 18.6 us  [the longest x43 18.6 us: shift(): return lax.ppermute(array, axis, [(j, (j + by) % n) for j in range(n)])]
    dot_general x6 -> x0, matrix products: 17.4 us -> none  [the longest x5 13.9 us: shards(): jnp.dot(scaled_in, shard_piece.reshape(shard_piece.shape[0], -1), preferr...]
    unnamed x36 -> x63, local copies, waits for them, and re-layouts: 6.01 us -> 13.8 us
    all_to_all x1 -> x0, waiting for transfers between devices: 6.96 us -> none  [summed_on_arrival(): lax.all_to_all(parts, axis, split_axis=0, concat_axis=0, tiled=True)]
    pallas_call x0 -> x4, Pallas kernels: none -> 5.39 us  [call(): pl.pallas_call(kernel, out_shape=out_shape, in_specs=[in_smem if a.dtype...]
    all_to_all x1 -> x0, starting transfers between devices: 3.98 us -> none  [summed_on_arrival(): lax.all_to_all(parts, axis, split_axis=0, concat_axis=0, tiled=True)]
  transfers between devices with their start and end apart: 3 -> 44, of which waited for: 3 -> 7; matrix products, arithmetic and copies ran while one was open for 12% -> 15% of each run, Pallas kernels for 0% -> 3%
where the time goes in v1:
time: 125 us; the launch traced here: 124 us
  starting transfers between devices  69.9 us (56%)
  waiting for transfers between devices  18.6 us (15%)
  local copies, waits for them, and re-layouts  16.9 us (14%)
  other arithmetic  6.16 us (5%)
  matrix products  5.73 us (5%)
  Pallas kernels  5.39 us (4%)
    ppermute x43, starting transfers between devices, shift(): return lax.ppermute(array, axis, [(j, (j + by) % n) for j in range(n)])  69.2 us
    ppermute x43, waiting for transfers between devices, shift(): return lax.ppermute(array, axis, [(j, (j + by) % n) for j in range(n)])  18.6 us
    unnamed x63, local copies, waits for them, and re-layouts  13.8 us
    pallas_call x4, Pallas kernels, call(): pl.pallas_call(kernel, out_shape=out_shape, in_specs=[in_smem if a.dtype...  5.39 us
    dot_general x1, matrix products, fold_pending(): jnp.einsum('sphd,sphe->shde', weighted_keys, value_rows, precision=highest)  3.7 us
  transfers between devices with their start and end apart: 44, of which 7 were waited for; matrix products, arithmetic and copies ran while one was open for 15% of the time, Pallas kernels for 3%

profile of v1, /device:TPU:1, one launch (start us, length us, event | category | flops | bytes accessed | tf_op | source)
XLA Modules:
  0.0 123.9 jit_solution(3087196922493231166)
XLA Ops:
  4.8 2.5 %collective-permute-start.3 = (bf16[64,2056]{1,0:T(8,128)(2,1)S(1)}, bf16[64,2056]{1,0:T(8,128)(2,1)S(1)}, u32[]{:S(2)}, u32[]{:S(2)}) collective-permute-start(bf16[64,2056]{1,0:T(8,128)(2,1)S(1)} %shard_map.193.refs_4_), channel_id=1, source_target_pairs={{0,32},{32,64},{64,96},{96,128},{128,160},{160,192},{192,224},{224... | collective-permute-start | bytes 789512 | tf_op jit(solution)/shard_map/ppermute | solution.py:22
  7.4 4.0 %collective-permute-start.7 = (bf16[64,2056]{1,0:T(8,128)(2,1)S(1)}, bf16[64,2056]{1,0:T(8,128)(2,1)S(1)}, u32[]{:S(2)}, u32[]{:S(2)}) collective-permute-start(bf16[64,2056]{1,0:T(8,128)(2,1)S(1)} %shard_map.193.refs_4_), channel_id=1, source_target_pairs={{0,224},{32,0},{64,32},{96,64},{128,96},{160,128},{192,160},{224,1... | collective-permute-start | bytes 789512 | tf_op jit(solution)/shard_map/ppermute | solution.py:22
  13.4 1.2 copy.130
  16.6 1.4 %collective-permute-start = (bf16[48,1024]{1,0:T(8,128)(2,1)S(1)}, bf16[48,1024]{1,0:T(8,128)(2,1)S(1)}, u32[]{:S(2)}, u32[]{:S(2)}) collective-permute-start(bf16[48,1024]{1,0:T(8,128)(2,1)S(1)} %get-tuple-element.37), channel_id=1, source_target_pairs={{0,8},{8,16},{16,24},{24,0},{1,9},{9,17},{17,25},{25,1},{2,10},{10... | collective-permute-start | bytes 294920 | tf_op jit(solution)/shard_map/ppermute | solution.py:22
  18.0 1.3 %collective-permute-start.26 = (bf16[256,128]{1,0:T(8,128)(2,1)S(1)}, bf16[256,128]{1,0:T(8,128)(2,1)S(1)}, u32[]{:S(2)}, u32[]{:S(2)}) collective-permute-start(bf16[256,128]{1,0:T(8,128)(2,1)S(1)} %collective-permute-done.25), channel_id=1, source_target_pairs={{0,8},{8,16},{16,24},{24,0},{1,9},{9,17},{17,25},{25,1},{2,10},{10... | collective-permute-start | bytes 196616 | tf_op jit(solution)/shard_map/ppermute | solution.py:22
  19.3 5.7 %collective-permute-start.4 = (bf16[64,2056]{1,0:T(8,128)(2,1)S(1)}, bf16[64,2056]{1,0:T(8,128)(2,1)S(1)}, u32[]{:S(2)}, u32[]{:S(2)}) collective-permute-start(bf16[64,2056]{1,0:T(8,128)(2,1)S(1)} %collective-permute-done.3.refs_5_), channel_id=1, source_target_pairs={{0,32},{32,64},{64,96},{96,128},{128,160},{160,192},{192,224},{224... | collective-permute-start | bytes 789512 | tf_op jit(solution)/shard_map/ppermute | solution.py:22
  25.1 2.6 %collective-permute-start.27 = (bf16[256,128]{1,0:T(8,128)(2,1)S(1)}, bf16[256,128]{1,0:T(8,128)(2,1)S(1)}, u32[]{:S(2)}, u32[]{:S(2)}) collective-permute-start(bf16[256,128]{1,0:T(8,128)(2,1)S(1)} %collective-permute-done.25), channel_id=1, source_target_pairs={{0,16},{8,24},{16,0},{24,8},{1,17},{9,25},{17,1},{25,9},{2,18},{10... | collective-permute-start | bytes 196616 | tf_op jit(solution)/shard_map/ppermute | solution.py:22
  27.7 2.1 %collective-permute-done.27 = bf16[256,128]{1,0:T(8,128)(2,1)S(1)} collective-permute-done((bf16[256,128]{1,0:T(8,128)(2,1)S(1)}, bf16[256,128]{1,0:T(8,128)(2,1)S(1)}, u32[]{:S(2)}, u32[]{:S(2)}) %collective-permute-start.27) | collective-permute-done | bytes 65568 | tf_op jit(solution)/shard_map/ppermute | solution.py:22
  29.8 1.4 %collective-permute-start.28 = (bf16[256,128]{1,0:T(8,128)(2,1)S(1)}, bf16[256,128]{1,0:T(8,128)(2,1)S(1)}, u32[]{:S(2)}, u32[]{:S(2)}) collective-permute-start(bf16[256,128]{1,0:T(8,128)(2,1)S(1)} %collective-permute-done.25), channel_id=1, source_target_pairs={{0,24},{8,0},{16,8},{24,16},{1,25},{9,1},{17,9},{25,17},{2,26},{10... | collective-permute-start | bytes 196616 | tf_op jit(solution)/shard_map/ppermute | solution.py:22
  31.2 1.7 %collective-permute-start.1 = (bf16[48,1024]{1,0:T(8,128)(2,1)S(1)}, bf16[48,1024]{1,0:T(8,128)(2,1)S(1)}, u32[]{:S(2)}, u32[]{:S(2)}) collective-permute-start(bf16[48,1024]{1,0:T(8,128)(2,1)S(1)} %get-tuple-element.36), channel_id=1, source_target_pairs={{0,16},{8,24},{16,0},{24,8},{1,17},{9,25},{17,1},{25,9},{2,18},{10... | collective-permute-start | bytes 294920 | tf_op jit(solution)/shard_map/ppermute | solution.py:22
  33.2 2.6 %collective-permute-start.2 = (bf16[48,1024]{1,0:T(8,128)(2,1)S(1)}, bf16[48,1024]{1,0:T(8,128)(2,1)S(1)}, u32[]{:S(2)}, u32[]{:S(2)}) collective-permute-start(bf16[48,1024]{1,0:T(8,128)(2,1)S(1)} %get-tuple-element.35), channel_id=1, source_target_pairs={{0,24},{8,0},{16,8},{24,16},{1,25},{9,1},{17,9},{25,17},{2,26},{10... | collective-permute-start | bytes 294920 | tf_op jit(solution)/shard_map/ppermute | solution.py:22
  35.8 5.9 %collective-permute-start.8 = (bf16[64,2056]{1,0:T(8,128)(2,1)S(1)}, bf16[64,2056]{1,0:T(8,128)(2,1)S(1)}, u32[]{:S(2)}, u32[]{:S(2)}) collective-permute-start(bf16[64,2056]{1,0:T(8,128)(2,1)S(1)} %collective-permute-done.7.refs_11_), channel_id=1, source_target_pairs={{0,224},{32,0},{64,32},{96,64},{128,96},{160,128},{192,160},{224,1... | collective-permute-start | bytes 789512 | tf_op jit(solution)/shard_map/ppermute | solution.py:22
  43.0 2.7 %collective-permute-start.33 = (bf16[256,512]{1,0:T(8,128)(2,1)S(1)}, bf16[256,512]{1,0:T(8,128)(2,1)}, u32[]{:S(2)}, u32[]{:S(2)}) collective-permute-start(bf16[256,512]{1,0:T(8,128)(2,1)S(1)} %constant_dynamic-update-slice_fusion.refs_5_), channel_id=1, source_target_pairs={{0,224},{32,0},{64,32},{96,64},{128,96},{160,128},{192,160},{224,1... | collective-permute-start | bytes 786440 | tf_op jit(solution)/shard_map/ppermute | solution.py:22
  45.7 7.8 %collective-permute-start.11 = (bf16[64,2056]{1,0:T(8,128)(2,1)S(1)}, bf16[64,2056]{1,0:T(8,128)(2,1)S(1)}, u32[]{:S(2)}, u32[]{:S(2)}) collective-permute-start(bf16[64,2056]{1,0:T(8,128)(2,1)S(1)} %collective-permute-done.3.refs_5_), channel_id=1, source_target_pairs={{0,4},{4,0},{1,5},{5,1},{2,6},{6,2},{3,7},{7,3},{8,12},{12,8},{9,1... | collective-permute-start | bytes 789512 | tf_op jit(solution)/shard_map/ppermute | solution.py:22
  53.5 6.1 %collective-permute-start.17 = (bf16[64,2056]{1,0:T(8,128)(2,1)S(1)}, bf16[64,2056]{1,0:T(8,128)(2,1)S(1)}, u32[]{:S(2)}, u32[]{:S(2)}) collective-permute-start(bf16[64,2056]{1,0:T(8,128)(2,1)S(1)} %collective-permute-done.7.refs_11_), channel_id=1, source_target_pairs={{0,4},{4,0},{1,5},{5,1},{2,6},{6,2},{3,7},{7,3},{8,12},{12,8},{9,1... | collective-permute-start | bytes 789512 | tf_op jit(solution)/shard_map/ppermute | solution.py:22
  59.7 2.7 %collective-permute-start.9 = (bf16[64,2056]{1,0:T(8,128)(2,1)S(1)}, bf16[64,2056]{1,0:T(8,128)(2,1)S(1)}, u32[]{:S(2)}, u32[]{:S(2)}) collective-permute-start(bf16[64,2056]{1,0:T(8,128)(2,1)S(1)} %collective-permute-done.8.refs_10_), channel_id=1, source_target_pairs={{0,224},{32,0},{64,32},{96,64},{128,96},{160,128},{192,160},{224,1... | collective-permute-start | bytes 789512 | tf_op jit(solution)/shard_map/ppermute | solution.py:22
  64.4 4.4 %collective-permute-done.30.refs_7_ = bf16[256,512]{1,0:T(8,128)(2,1)S(1)} collective-permute-done((bf16[256,512]{1,0:T(8,128)(2,1)}, bf16[256,512]{1,0:T(8,128)(2,1)S(1)}, u32[]{:S(2)}, u32[]{:S(2)}) %collective-permute-start.30) | collective-permute-done | bytes 262176 | tf_op jit(solution)/shard_map/ppermute | solution.py:22
  68.9 1.5 %collective-permute-start.13 = (bf16[64,2056]{1,0:T(8,128)(2,1)S(1)}, bf16[64,2056]{1,0:T(8,128)(2,1)}, u32[]{:S(2)}, u32[]{:S(2)}) collective-permute-start(bf16[64,2056]{1,0:T(8,128)(2,1)S(1)} %collective-permute-done.5.refs_7_), channel_id=1, source_target_pairs={{0,4},{4,0},{1,5},{5,1},{2,6},{6,2},{3,7},{7,3},{8,12},{12,8},{9,1... | collective-permute-start | bytes 789512 | tf_op jit(solution)/shard_map/ppermute | solution.py:22
  70.4 4.4 %collective-permute-done.6.refs_8_ = bf16[64,2056]{1,0:T(8,128)(2,1)S(1)} collective-permute-done((bf16[64,2056]{1,0:T(8,128)(2,1)S(1)}, bf16[64,2056]{1,0:T(8,128)(2,1)S(1)}, u32[]{:S(2)}, u32[]{:S(2)}) %collective-permute-start.6) | collective-permute-done | bytes 263200 | tf_op jit(solution)/shard_map/ppermute | solution.py:22
  78.6 1.5 %collective-permute-start.31 = (bf16[256,512]{1,0:T(8,128)(2,1)}, bf16[256,512]{1,0:T(8,128)(2,1)}, u32[]{:S(2)}, u32[]{:S(2)}) collective-permute-start(bf16[256,512]{1,0:T(8,128)(2,1)} %copy-done.1), channel_id=1, source_target_pairs={{0,32},{32,64},{64,96},{96,128},{128,160},{160,192},{192,224},{224... | collective-permute-start | bytes 786440 | tf_op jit(solution)/shard_map/ppermute | solution.py:22
  82.7 2.5 %shard_map.194 = bf16[4,48,2064]{2,1,0:T(8,128)(2,1)S(1)} custom-call(bf16[48,1024]{1,0:T(8,128)(2,1)S(1)} %get-tuple-element.38.refs_0_, bf16[48,1024]{1,0:T(8,128)(2,1)S(1)} %copy-done.4, bf16[48,1024]{1,0:T(8,128)(2,1)S(1)} %copy-done.6, bf16[48,1024]{1,0:T(8,128)(2,1)S(1)} %copy-done.8, bf16[64,2056]{1,0:T(8,128)(2,1)S(1)} %shard_map.193.refs_4_, ...), custom_call_target="tpu_custom_call" | custom-call | flops 805306368 | bytes 5396480 | tf_op jit(solution)/shard_map/pallas_call | solution.py:45
  85.5 1.4 %collective-permute-start.20 = (bf16[48,2064]{1,0:T(8,128)(2,1)S(1)}, bf16[48,2064]{1,0:T(8,128)(2,1)S(1)}, u32[]{:S(2)}, u32[]{:S(2)}) collective-permute-start(bf16[48,2064]{1,0:T(8,128)(2,1)S(1)} %get-tuple-element.33), channel_id=1, source_target_pairs={{0,8},{8,16},{16,24},{24,0},{1,9},{9,17},{17,25},{25,1},{2,10},{10... | collective-permute-start | bytes 594440 | tf_op jit(solution)/shard_map/ppermute | solution.py:22
  88.9 2.7 %collective-permute-done.18 = bf16[48,2064]{1,0:T(8,128)(2,1)S(1)} collective-permute-done((bf16[48,2064]{1,0:T(8,128)(2,1)S(1)}, bf16[48,2064]{1,0:T(8,128)(2,1)S(1)}, u32[]{:S(2)}, u32[]{:S(2)}) %collective-permute-start.18) | collective-permute-done | bytes 198176 | tf_op jit(solution)/shard_map/ppermute | solution.py:22
  91.5 2.4 %collective-permute-start.43 = (bf16[256,512]{1,0:T(8,128)(2,1)}, bf16[256,512]{1,0:T(8,128)(2,1)S(1)}, u32[]{:S(2)}, u32[]{:S(2)}) collective-permute-start(bf16[256,512]{1,0:T(8,128)(2,1)} %collective-permute-done.33.refs_12_), channel_id=1, source_target_pairs={{0,4},{4,0},{1,5},{5,1},{2,6},{6,2},{3,7},{7,3},{8,12},{12,8},{9,1... | collective-permute-start | bytes 786440 | tf_op jit(solution)/shard_map/ppermute | solution.py:22
  95.0 3.5 %collective-permute-done.20 = bf16[48,2064]{1,0:T(8,128)(2,1)S(1)} collective-permute-done((bf16[48,2064]{1,0:T(8,128)(2,1)S(1)}, bf16[48,2064]{1,0:T(8,128)(2,1)S(1)}, u32[]{:S(2)}, u32[]{:S(2)}) %collective-permute-start.20) | collective-permute-done | bytes 198176 | tf_op jit(solution)/shard_map/ppermute | solution.py:22
  99.2 1.4 %reduce_window_sum.18 = f32[8,6,4]{1,2,0:T(4,128)S(1)} reduce-window(f32[8,6,4]{1,2,0:T(4,128)S(1)} %get-tuple-element.52, f32[]{:T(128)} %constant.44.clone.1), window={size=1x6x1 pad=0_0x5_0x0_0}, to_apply=%region_1.2 | reduce-window | flops 960 | bytes 1540 | tf_op jit(solution)/shard_map/jit(cumsum)/reduce_window_sum | solution.py:136
  101.4 1.4 %reduce_window_sum.17 = f32[8,6,4]{1,2,0:T(4,128)S(1)} reduce-window(f32[8,6,4]{1,2,0:T(4,128)S(1)} %get-tuple-element.51, f32[]{:T(128)} %constant.44.clone.1), window={size=1x6x1 pad=0_0x5_0x0_0}, to_apply=%region_0.1 | reduce-window | flops 960 | bytes 1540 | tf_op jit(solution)/shard_map/jit(cumsum)/reduce_window_sum | solution.py:153
  104.4 3.7 %multiply_add_fusion = f32[8,4,128,128]{3,2,1,0:T(8,128)S(1)} fusion(f32[8,4,128,128]{3,2,1,0:T(8,128)} %param.27, f32[8,4]{1,0:T(8,128)S(1)} %get-tuple-element.28, f32[8,6,4,128]{3,0,2,1:T(8,128)S(1)} %copy-done.15, bf16[8,6,4,128]{3,0,2,1:T(8,128)(2,1)S(1)} %bitcast.103, f32[8,6,4]{1,2,0:T(4,128)S(1)} %exponential_multiply_fusion), kind=kOutput, calls=%fused_computation | convolution fusion | flops 38821888 | bytes 4342656 | tf_op jit(solution)/shard_map/sphd,sphe->shde/dot_general | solution.py:143
  108.2 1.3 %copy-done.14 = f32[8,4,128,128]{3,2,1,0:T(8,128)} copy-done((f32[8,4,128,128]{3,2,1,0:T(8,128)}, f32[8,4,128,128]{3,2,1,0:T(8,128)S(1)}, u32[]{:S(2)}) %copy-start.14) | copy-done | bytes 2097176
  113.2 3.4 %collective-permute-start.21 = (bf16[48,512]{1,0:T(8,128)(2,1)S(1)}, bf16[48,512]{1,0:T(8,128)(2,1)S(1)}, u32[]{:S(2)}, u32[]{:S(2)}) collective-permute-start(bf16[48,512]{1,0:T(8,128)(2,1)S(1)} %bitcast.104), channel_id=1, source_target_pairs={{0,1},{1,2},{2,3},{3,0},{4,5},{5,6},{6,7},{7,4},{8,9},{9,10},{10,1... | collective-permute-start | bytes 147464 | tf_op jit(solution)/shard_map/ppermute | solution.py:22
  116.7 2.7 %collective-permute-start.23 = (bf16[48,512]{1,0:T(8,128)(2,1)S(1)}, bf16[48,512]{1,0:T(8,128)(2,1)S(1)}, u32[]{:S(2)}, u32[]{:S(2)}) collective-permute-start(bf16[48,512]{1,0:T(8,128)(2,1)S(1)} %bitcast.106), channel_id=1, source_target_pairs={{0,3},{1,0},{2,1},{3,2},{4,7},{5,4},{6,5},{7,6},{8,11},{9,8},{10,9... | collective-permute-start | bytes 147464 | tf_op jit(solution)/shard_map/ppermute | solution.py:22
  121.1 2.0 %shard_map.195 = bf16[48,1024]{1,0:T(8,128)(2,1)S(1)} custom-call(s32[4]{0:T(128)S(1)} %pad_add_fusion.place.refs_0_, bf16[48,512]{1,0:T(8,128)(2,1)S(1)} %bitcast.107, bf16[48,512]{1,0:T(8,128)(2,1)S(1)} %collective-permute-done.21.refs_2_, bf16[48,512]{1,0:T(8,128)(2,1)S(1)} %collective-permute-done.22.refs_3_, ...), custom_call_target="tpu_custom_call" | custom-call | flops 201326592 | bytes 4489232 | tf_op jit(solution)/shard_map/pallas_call | solution.py:45
  (172 shorter events, 30.8 us)
Async XLA Ops:
  4.8 14.5 %collective-permute-start.3 = (bf16[64,2056]{1,0:T(8,128)(2,1)S(1)}, bf16[64,2056]{1,0:T(8,128)(2,1)S(1)}, u32[]{:S(2)}, u32[]{:S(2)}) collective-permute-start(bf16[64,2056]{1,0:T(8,128)(2,1)S(1)} %shard_map.193.refs_4_), channel_id=1, source_target_pairs={{0,32},{32,64},{64,96},{96,128},{128,160},{160,192},{192,224},{224... | collective-permute-start | bytes 789512 | tf_op jit(solution)/shard_map/ppermute | solution.py:22
  7.4 28.4 %collective-permute-start.7 = (bf16[64,2056]{1,0:T(8,128)(2,1)S(1)}, bf16[64,2056]{1,0:T(8,128)(2,1)S(1)}, u32[]{:S(2)}, u32[]{:S(2)}) collective-permute-start(bf16[64,2056]{1,0:T(8,128)(2,1)S(1)} %shard_map.193.refs_4_), channel_id=1, source_target_pairs={{0,224},{32,0},{64,32},{96,64},{128,96},{160,128},{192,160},{224,1... | collective-permute-start | bytes 789512 | tf_op jit(solution)/shard_map/ppermute | solution.py:22
  11.4 34.3 %collective-permute-start.10 = (bf16[64,2056]{1,0:T(8,128)(2,1)S(1)}, bf16[64,2056]{1,0:T(8,128)(2,1)S(1)}, u32[]{:S(2)}, u32[]{:S(2)}) collective-permute-start(bf16[64,2056]{1,0:T(8,128)(2,1)S(1)} %shard_map.193.refs_4_), channel_id=1, source_target_pairs={{0,4},{4,0},{1,5},{5,1},{2,6},{6,2},{3,7},{7,3},{8,12},{12,8},{9,1... | collective-permute-start | bytes 789512 | tf_op jit(solution)/shard_map/ppermute | solution.py:22
  16.6 14.5 %collective-permute-start = (bf16[48,1024]{1,0:T(8,128)(2,1)S(1)}, bf16[48,1024]{1,0:T(8,128)(2,1)S(1)}, u32[]{:S(2)}, u32[]{:S(2)}) collective-permute-start(bf16[48,1024]{1,0:T(8,128)(2,1)S(1)} %get-tuple-element.37), channel_id=1, source_target_pairs={{0,8},{8,16},{16,24},{24,0},{1,9},{9,17},{17,25},{25,1},{2,10},{10... | collective-permute-start | bytes 294920 | tf_op jit(solution)/shard_map/ppermute | solution.py:22
  18.0 7.0 %collective-permute-start.26 = (bf16[256,128]{1,0:T(8,128)(2,1)S(1)}, bf16[256,128]{1,0:T(8,128)(2,1)S(1)}, u32[]{:S(2)}, u32[]{:S(2)}) collective-permute-start(bf16[256,128]{1,0:T(8,128)(2,1)S(1)} %collective-permute-done.25), channel_id=1, source_target_pairs={{0,8},{8,16},{16,24},{24,0},{1,9},{9,17},{17,25},{25,1},{2,10},{10... | collective-permute-start | bytes 196616 | tf_op jit(solution)/shard_map/ppermute | solution.py:22
  19.3 22.4 %collective-permute-start.4 = (bf16[64,2056]{1,0:T(8,128)(2,1)S(1)}, bf16[64,2056]{1,0:T(8,128)(2,1)S(1)}, u32[]{:S(2)}, u32[]{:S(2)}) collective-permute-start(bf16[64,2056]{1,0:T(8,128)(2,1)S(1)} %collective-permute-done.3.refs_5_), channel_id=1, source_target_pairs={{0,32},{32,64},{64,96},{96,128},{128,160},{160,192},{192,224},{224... | collective-permute-start | bytes 789512 | tf_op jit(solution)/shard_map/ppermute | solution.py:22
  31.2 10.5 %collective-permute-start.1 = (bf16[48,1024]{1,0:T(8,128)(2,1)S(1)}, bf16[48,1024]{1,0:T(8,128)(2,1)S(1)}, u32[]{:S(2)}, u32[]{:S(2)}) collective-permute-start(bf16[48,1024]{1,0:T(8,128)(2,1)S(1)} %get-tuple-element.36), channel_id=1, source_target_pairs={{0,16},{8,24},{16,0},{24,8},{1,17},{9,25},{17,1},{25,9},{2,18},{10... | collective-permute-start | bytes 294920 | tf_op jit(solution)/shard_map/ppermute | solution.py:22
  33.2 9.2 %collective-permute-start.2 = (bf16[48,1024]{1,0:T(8,128)(2,1)S(1)}, bf16[48,1024]{1,0:T(8,128)(2,1)S(1)}, u32[]{:S(2)}, u32[]{:S(2)}) collective-permute-start(bf16[48,1024]{1,0:T(8,128)(2,1)S(1)} %get-tuple-element.35), channel_id=1, source_target_pairs={{0,24},{8,0},{16,8},{24,16},{1,25},{9,1},{17,9},{25,17},{2,26},{10... | collective-permute-start | bytes 294920 | tf_op jit(solution)/shard_map/ppermute | solution.py:22
  35.8 23.9 %collective-permute-start.8 = (bf16[64,2056]{1,0:T(8,128)(2,1)S(1)}, bf16[64,2056]{1,0:T(8,128)(2,1)S(1)}, u32[]{:S(2)}, u32[]{:S(2)}) collective-permute-start(bf16[64,2056]{1,0:T(8,128)(2,1)S(1)} %collective-permute-done.7.refs_11_), channel_id=1, source_target_pairs={{0,224},{32,0},{64,32},{96,64},{128,96},{160,128},{192,160},{224,1... | collective-permute-start | bytes 789512 | tf_op jit(solution)/shard_map/ppermute | solution.py:22
  41.7 20.6 %collective-permute-start.5 = (bf16[64,2056]{1,0:T(8,128)(2,1)S(1)}, bf16[64,2056]{1,0:T(8,128)(2,1)S(1)}, u32[]{:S(2)}, u32[]{:S(2)}) collective-permute-start(bf16[64,2056]{1,0:T(8,128)(2,1)S(1)} %collective-permute-done.4.refs_6_), channel_id=1, source_target_pairs={{0,32},{32,64},{64,96},{96,128},{128,160},{160,192},{192,224},{224... | collective-permute-start | bytes 789512 | tf_op jit(solution)/shard_map/ppermute | solution.py:22
  42.4 11.1 %collective-permute-start.29 = (bf16[256,512]{1,0:T(8,128)(2,1)S(1)}, bf16[256,512]{1,0:T(8,128)(2,1)}, u32[]{:S(2)}, u32[]{:S(2)}) collective-permute-start(bf16[256,512]{1,0:T(8,128)(2,1)S(1)} %constant_dynamic-update-slice_fusion.refs_5_), channel_id=1, source_target_pairs={{0,32},{32,64},{64,96},{96,128},{128,160},{160,192},{192,224},{224... | collective-permute-start | bytes 786440 | tf_op jit(solution)/shard_map/ppermute | solution.py:22
  43.0 16.6 %collective-permute-start.33 = (bf16[256,512]{1,0:T(8,128)(2,1)S(1)}, bf16[256,512]{1,0:T(8,128)(2,1)}, u32[]{:S(2)}, u32[]{:S(2)}) collective-permute-start(bf16[256,512]{1,0:T(8,128)(2,1)S(1)} %constant_dynamic-update-slice_fusion.refs_5_), channel_id=1, source_target_pairs={{0,224},{32,0},{64,32},{96,64},{128,96},{160,128},{192,160},{224,1... | collective-permute-start | bytes 786440 | tf_op jit(solution)/shard_map/ppermute | solution.py:22
  45.7 18.0 %collective-permute-start.11 = (bf16[64,2056]{1,0:T(8,128)(2,1)S(1)}, bf16[64,2056]{1,0:T(8,128)(2,1)S(1)}, u32[]{:S(2)}, u32[]{:S(2)}) collective-permute-start(bf16[64,2056]{1,0:T(8,128)(2,1)S(1)} %collective-permute-done.3.refs_5_), channel_id=1, source_target_pairs={{0,4},{4,0},{1,5},{5,1},{2,6},{6,2},{3,7},{7,3},{8,12},{12,8},{9,1... | collective-permute-start | bytes 789512 | tf_op jit(solution)/shard_map/ppermute | solution.py:22
  53.5 10.8 %collective-permute-start.17 = (bf16[64,2056]{1,0:T(8,128)(2,1)S(1)}, bf16[64,2056]{1,0:T(8,128)(2,1)S(1)}, u32[]{:S(2)}, u32[]{:S(2)}) collective-permute-start(bf16[64,2056]{1,0:T(8,128)(2,1)S(1)} %collective-permute-done.7.refs_11_), channel_id=1, source_target_pairs={{0,4},{4,0},{1,5},{5,1},{2,6},{6,2},{3,7},{7,3},{8,12},{12,8},{9,1... | collective-permute-start | bytes 789512 | tf_op jit(solution)/shard_map/ppermute | solution.py:22
  59.6 9.2 %collective-permute-start.30 = (bf16[256,512]{1,0:T(8,128)(2,1)}, bf16[256,512]{1,0:T(8,128)(2,1)S(1)}, u32[]{:S(2)}, u32[]{:S(2)}) collective-permute-start(bf16[256,512]{1,0:T(8,128)(2,1)} %collective-permute-done.29.refs_6_), channel_id=1, source_target_pairs={{0,32},{32,64},{64,96},{96,128},{128,160},{160,192},{192,224},{224... | collective-permute-start | bytes 786440 | tf_op jit(solution)/shard_map/ppermute | solution.py:22
  59.7 10.7 %collective-permute-start.9 = (bf16[64,2056]{1,0:T(8,128)(2,1)S(1)}, bf16[64,2056]{1,0:T(8,128)(2,1)S(1)}, u32[]{:S(2)}, u32[]{:S(2)}) collective-permute-start(bf16[64,2056]{1,0:T(8,128)(2,1)S(1)} %collective-permute-done.8.refs_10_), channel_id=1, source_target_pairs={{0,224},{32,0},{64,32},{96,64},{128,96},{160,128},{192,160},{224,1... | collective-permute-start | bytes 789512 | tf_op jit(solution)/shard_map/ppermute | solution.py:22
  62.3 12.5 %collective-permute-start.6 = (bf16[64,2056]{1,0:T(8,128)(2,1)S(1)}, bf16[64,2056]{1,0:T(8,128)(2,1)S(1)}, u32[]{:S(2)}, u32[]{:S(2)}) collective-permute-start(bf16[64,2056]{1,0:T(8,128)(2,1)S(1)} %collective-permute-done.5.refs_7_), channel_id=1, source_target_pairs={{0,32},{32,64},{64,96},{96,128},{128,160},{160,192},{192,224},{224... | collective-permute-start | bytes 789512 | tf_op jit(solution)/shard_map/ppermute | solution.py:22
  63.7 14.9 %collective-permute-start.12 = (bf16[64,2056]{1,0:T(8,128)(2,1)S(1)}, bf16[64,2056]{1,0:T(8,128)(2,1)}, u32[]{:S(2)}, u32[]{:S(2)}) collective-permute-start(bf16[64,2056]{1,0:T(8,128)(2,1)S(1)} %collective-permute-done.4.refs_6_), channel_id=1, source_target_pairs={{0,4},{4,0},{1,5},{5,1},{2,6},{6,2},{3,7},{7,3},{8,12},{12,8},{9,1... | collective-permute-start | bytes 789512 | tf_op jit(solution)/shard_map/ppermute | solution.py:22
  64.3 14.2 %collective-permute-start.16 = (bf16[64,2056]{1,0:T(8,128)(2,1)S(1)}, bf16[64,2056]{1,0:T(8,128)(2,1)}, u32[]{:S(2)}, u32[]{:S(2)}) collective-permute-start(bf16[64,2056]{1,0:T(8,128)(2,1)S(1)} %collective-permute-done.8.refs_10_), channel_id=1, source_target_pairs={{0,4},{4,0},{1,5},{5,1},{2,6},{6,2},{3,7},{7,3},{8,12},{12,8},{9,1... | collective-permute-start | bytes 789512 | tf_op jit(solution)/shard_map/ppermute | solution.py:22
  68.9 11.2 %collective-permute-start.13 = (bf16[64,2056]{1,0:T(8,128)(2,1)S(1)}, bf16[64,2056]{1,0:T(8,128)(2,1)}, u32[]{:S(2)}, u32[]{:S(2)}) collective-permute-start(bf16[64,2056]{1,0:T(8,128)(2,1)S(1)} %collective-permute-done.5.refs_7_), channel_id=1, source_target_pairs={{0,4},{4,0},{1,5},{5,1},{2,6},{6,2},{3,7},{7,3},{8,12},{12,8},{9,1... | collective-permute-start | bytes 789512 | tf_op jit(solution)/shard_map/ppermute | solution.py:22
  70.3 9.7 %collective-permute-start.15 = (bf16[64,2056]{1,0:T(8,128)(2,1)S(1)}, bf16[64,2056]{1,0:T(8,128)(2,1)}, u32[]{:S(2)}, u32[]{:S(2)}) collective-permute-start(bf16[64,2056]{1,0:T(8,128)(2,1)S(1)} %collective-permute-done.9.refs_9_), channel_id=1, source_target_pairs={{0,4},{4,0},{1,5},{5,1},{2,6},{6,2},{3,7},{7,3},{8,12},{12,8},{9,1... | collective-permute-start | bytes 789512 | tf_op jit(solution)/shard_map/ppermute | solution.py:22
  78.6 8.4 %collective-permute-start.34 = (bf16[256,512]{1,0:T(8,128)(2,1)}, bf16[256,512]{1,0:T(8,128)(2,1)}, u32[]{:S(2)}, u32[]{:S(2)}) collective-permute-start(bf16[256,512]{1,0:T(8,128)(2,1)} %collective-permute-done.33.refs_12_), channel_id=1, source_target_pairs={{0,224},{32,0},{64,32},{96,64},{128,96},{160,128},{192,160},{224,1... | collective-permute-start | bytes 786440 | tf_op jit(solution)/shard_map/ppermute | solution.py:22
  78.6 9.6 %collective-permute-start.31 = (bf16[256,512]{1,0:T(8,128)(2,1)}, bf16[256,512]{1,0:T(8,128)(2,1)}, u32[]{:S(2)}, u32[]{:S(2)}) collective-permute-start(bf16[256,512]{1,0:T(8,128)(2,1)} %copy-done.1), channel_id=1, source_target_pairs={{0,32},{32,64},{64,96},{96,128},{128,160},{160,192},{192,224},{224... | collective-permute-start | bytes 786440 | tf_op jit(solution)/shard_map/ppermute | solution.py:22
  85.4 8.6 %collective-permute-start.19 = (bf16[48,2064]{1,0:T(8,128)(2,1)S(1)}, bf16[48,2064]{1,0:T(8,128)(2,1)S(1)}, u32[]{:S(2)}, u32[]{:S(2)}) collective-permute-start(bf16[48,2064]{1,0:T(8,128)(2,1)S(1)} %get-tuple-element.34), channel_id=1, source_target_pairs={{0,16},{8,24},{16,0},{24,8},{1,17},{9,25},{17,1},{25,9},{2,18},{10... | collective-permute-start | bytes 594440 | tf_op jit(solution)/shard_map/ppermute | solution.py:22
  85.5 13.1 %collective-permute-start.20 = (bf16[48,2064]{1,0:T(8,128)(2,1)S(1)}, bf16[48,2064]{1,0:T(8,128)(2,1)S(1)}, u32[]{:S(2)}, u32[]{:S(2)}) collective-permute-start(bf16[48,2064]{1,0:T(8,128)(2,1)S(1)} %get-tuple-element.33), channel_id=1, source_target_pairs={{0,8},{8,16},{16,24},{24,0},{1,9},{9,17},{17,25},{25,1},{2,10},{10... | collective-permute-start | bytes 594440 | tf_op jit(solution)/shard_map/ppermute | solution.py:22
  86.9 24.0 %collective-permute-start.36 = (bf16[256,512]{1,0:T(8,128)(2,1)S(1)}, bf16[256,512]{1,0:T(8,128)(2,1)S(1)}, u32[]{:S(2)}, u32[]{:S(2)}) collective-permute-start(bf16[256,512]{1,0:T(8,128)(2,1)S(1)} %constant_dynamic-update-slice_fusion.refs_5_), channel_id=1, source_target_pairs={{0,4},{4,0},{1,5},{5,1},{2,6},{6,2},{3,7},{7,3},{8,12},{12,8},{9,1... | collective-permute-start | bytes 786440 | tf_op jit(solution)/shard_map/ppermute | solution.py:22
  88.1 23.7 %collective-permute-start.37 = (bf16[256,512]{1,0:T(8,128)(2,1)}, bf16[256,512]{1,0:T(8,128)(2,1)S(1)}, u32[]{:S(2)}, u32[]{:S(2)}) collective-permute-start(bf16[256,512]{1,0:T(8,128)(2,1)} %collective-permute-done.29.refs_6_), channel_id=1, source_target_pairs={{0,4},{4,0},{1,5},{5,1},{2,6},{6,2},{3,7},{7,3},{8,12},{12,8},{9,1... | collective-permute-start | bytes 786440 | tf_op jit(solution)/shard_map/ppermute | solution.py:22
  91.5 20.4 %collective-permute-start.43 = (bf16[256,512]{1,0:T(8,128)(2,1)}, bf16[256,512]{1,0:T(8,128)(2,1)S(1)}, u32[]{:S(2)}, u32[]{:S(2)}) collective-permute-start(bf16[256,512]{1,0:T(8,128)(2,1)} %collective-permute-done.33.refs_12_), channel_id=1, source_target_pairs={{0,4},{4,0},{1,5},{5,1},{2,6},{6,2},{3,7},{7,3},{8,12},{12,8},{9,1... | collective-permute-start | bytes 786440 | tf_op jit(solution)/shard_map/ppermute | solution.py:22
  94.0 18.4 %collective-permute-start.35 = (bf16[256,512]{1,0:T(8,128)(2,1)}, bf16[256,512]{1,0:T(8,128)(2,1)S(1)}, u32[]{:S(2)}, u32[]{:S(2)}) collective-permute-start(bf16[256,512]{1,0:T(8,128)(2,1)} %collective-permute-done.34.refs_11_), channel_id=1, source_target_pairs={{0,224},{32,0},{64,32},{96,64},{128,96},{160,128},{192,160},{224,1... | collective-permute-start | bytes 786440 | tf_op jit(solution)/shard_map/ppermute | solution.py:22
  98.6 14.1 %collective-permute-start.32 = (bf16[256,512]{1,0:T(8,128)(2,1)}, bf16[256,512]{1,0:T(8,128)(2,1)S(1)}, u32[]{:S(2)}, u32[]{:S(2)}) collective-permute-start(bf16[256,512]{1,0:T(8,128)(2,1)} %collective-permute-done.31.refs_8_), channel_id=1, source_target_pairs={{0,32},{32,64},{64,96},{96,128},{128,160},{160,192},{192,224},{224... | collective-permute-start | bytes 786440 | tf_op jit(solution)/shard_map/ppermute | solution.py:22
  112.4 7.5 %collective-permute-start.41 = (bf16[256,512]{1,0:T(8,128)(2,1)S(1)}, bf16[256,512]{1,0:T(8,128)(2,1)S(1)}, u32[]{:S(2)}, u32[]{:S(2)}) collective-permute-start(bf16[256,512]{1,0:T(8,128)(2,1)S(1)} %collective-permute-done.35.refs_10_), channel_id=1, source_target_pairs={{0,4},{4,0},{1,5},{5,1},{2,6},{6,2},{3,7},{7,3},{8,12},{12,8},{9,1... | collective-permute-start | bytes 786440 | tf_op jit(solution)/shard_map/ppermute | solution.py:22
  112.6 7.3 %collective-permute-start.40 = (bf16[256,512]{1,0:T(8,128)(2,1)S(1)}, bf16[256,512]{1,0:T(8,128)(2,1)S(1)}, u32[]{:S(2)}, u32[]{:S(2)}) collective-permute-start(bf16[256,512]{1,0:T(8,128)(2,1)S(1)} %collective-permute-done.32.refs_9_), channel_id=1, source_target_pairs={{0,4},{4,0},{1,5},{5,1},{2,6},{6,2},{3,7},{7,3},{8,12},{12,8},{9,1... | collective-permute-start | bytes 786440 | tf_op jit(solution)/shard_map/ppermute | solution.py:22
  (37 other events, 386.2 us)

commit v2 on v1

v2 whole, which is shorter than its diff:
```python
import functools

import jax
import jax.numpy as jnp
from jax import lax
from jax.experimental import pallas as pl
from jax.experimental.pallas import tpu as pltpu
from jax.sharding import Mesh
from jax.sharding import PartitionSpec as P

epsilon = 1e-06
very_low = -1e30
bf16 = jnp.bfloat16
f32 = jnp.float32
in_vmem = pl.BlockSpec(memory_space=pltpu.VMEM)
in_hbm = pl.BlockSpec(memory_space=pltpu.HBM)
in_smem = pl.BlockSpec(memory_space=pltpu.SMEM)


def shift(array, axis, by):
    n = lax.axis_size(axis)
    return lax.ppermute(array, axis, [(j, (j + by) % n) for j in range(n)])


def ring(chunk, axis):
    n = lax.axis_size(axis)
    chunks = [chunk] + [None] * (n - 1)
    ahead = behind = chunk
    for s in range(1, n // 2 + 1):
        ahead = shift(ahead, axis, 1)
        chunks[s] = ahead
        if n - s > s:
            behind = shift(behind, axis, -1)
            chunks[n - s] = behind
    return chunks


def direct(chunk, axis):
    return [chunk] + [shift(chunk, axis, s) for s in range(1, lax.axis_size(axis))]


def call(kernel, out_shape, specs, *args, flops=0, scratch=(), vmem=32):
    outs = jax.tree.leaves(out_shape)
    nbytes = sum(a.size * a.dtype.itemsize for a in (*args, *outs))
    return pl.pallas_call(
        kernel,
        out_shape=out_shape,
        in_specs=specs + [in_vmem] * (len(args) - len(specs)),
        out_specs=jax.tree.map(lambda _: in_vmem, out_shape),
        scratch_shapes=list(scratch),
        compiler_params=pltpu.CompilerParams(vmem_limit_bytes=vmem * 2**20),
        cost_estimate=pl.CostEstimate(flops=max(flops, 2 * nbytes), bytes_accessed=nbytes, transcendentals=0),
    )(*args)


def array(shape, dtype=f32):
    return jax.ShapeDtypeStruct(shape, dtype)


def pack_kernel(*refs):
    *ins, w_gates, w_mix, out, sems = refs
    at, copies = 0, []
    for i, ref in enumerate(ins):
        width = ref.shape[1]
        copies.append(pltpu.make_async_copy(ref, out.at[:, at : at + width], sems.at[i]))
        copies[-1].start()
        at += width
    out[:, at : at + w_mix.shape[0]] = w_mix[...].astype(f32).T.astype(bf16)
    out[:, at + w_mix.shape[0] :] = w_gates[...]
    for copy in copies:
        copy.wait()


def prep_kernel(nz, ny, place, tokens, gain, out, squares):
    z, y, c = place[0], place[1], place[2]
    width = tokens.shape[1]
    unit = width // (nz * ny)
    wide = tokens[...].astype(f32)
    squares[...] = jnp.sum(wide * wide, axis=-1, keepdims=True)
    for sz in range(nz):
        for sy in range(ny):
            block = lax.rem(z - sz + nz, nz) * ny + lax.rem(y + sy, ny)
            lanes = pl.ds(pl.multiple_of(block * unit, unit), unit)
            scaled = tokens[:, lanes].astype(f32) * gain[:, lanes]
            scaled = jnp.where(c == 1, pltpu.roll(scaled, unit // 2, 1), scaled)
            out[sy, :, sz * unit : (sz + 1) * unit] = scaled.astype(bf16)


def log_sigmoid(x):
    return jnp.minimum(x, 0.0) - jnp.log1p(jnp.exp(-jnp.abs(x)))


def over_lanes(small, size):
    rows, heads = small.shape
    return jnp.concatenate([jnp.broadcast_to(small[:, h : h + 1], (rows, size)) for h in range(heads)], axis=1)


def head_sums(wide, heads):
    size = wide.shape[1] // heads
    return jnp.concatenate(
        [jnp.sum(wide[:, h * size : (h + 1) * size], axis=1, keepdims=True) for h in range(heads)], axis=1
    )


def largest(parts):
    return functools.reduce(jnp.maximum, parts)


def fold_kernel(
    cell, norm, stabilizer, keys, values, gate_in, gate_keep, bias, accepted,
    cell_out, cell_low, norm_out, max_out, key_rows, value_rows,
):
    seqs, heads = stabilizer.shape
    size = cell.shape[-1]
    props = keys.shape[0] // seqs
    at = [slice(p * seqs, (p + 1) * seqs) for p in range(props)]
    held = jnp.broadcast_to(accepted[...], (seqs, heads))
    log_in, running, total = [], [], jnp.zeros((seqs, heads), f32)
    for p in range(props):
        log_in.append(jnp.where(held > p, gate_in[at[p]], very_low))
        total = total + jnp.where(held > p, log_sigmoid(gate_keep[at[p]] + bias[...]), 0.0)
        running.append(total)
    log_w = [total - running[p] + log_in[p] for p in range(props)]
    new_max = jnp.maximum(total + stabilizer[...], largest(log_w))
    carried = jnp.exp(total + stabilizer[...] - new_max)
    max_out[...] = new_max
    key_rows[...] = jnp.zeros_like(key_rows)
    value_rows[...] = jnp.zeros_like(value_rows)
    normer = over_lanes(carried, size) * norm[...]
    for p in range(props):
        weighted = over_lanes(jnp.exp(log_w[p] - new_max), size) * (keys[at[p]].astype(f32) * size**-0.5)
        value = values[at[p]].astype(f32)
        for h in range(heads):
            key_rows[h, at[p]] = weighted[:, h * size : (h + 1) * size]
            value_rows[h, at[p]] = value[:, h * size : (h + 1) * size]
        normer = normer + weighted
    norm_out[...] = normer
    padded = key_rows.shape[1] // seqs
    for s in range(seqs):
        for h in range(heads):
            k = key_rows[h, pl.ds(s, padded, stride=seqs), :]
            v = value_rows[h, pl.ds(s, padded, stride=seqs), :]
            high = k.astype(bf16).astype(f32)
            left = jnp.concatenate([high, k - high], axis=0).astype(bf16)
            right = jnp.concatenate([v, v], axis=0).astype(bf16)
            added = lax.dot_general(left, right, (((0,), (0,)), ((), ())), preferred_element_type=f32)
            new = carried[s : s + 1, h : h + 1] * cell[s * heads + h] + added
            cell_out[s * heads + h] = new
            cell_low[s * heads + h] = new.astype(bf16)


def read_kernel(model_width, *refs):
    parts, refs = refs[:-11], refs[-11:]
    squares, cell_low, norm, stabilizer, bias, gain, out, query_rows, prior_rows, key_rows, value_rows = refs
    seqs, heads = stabilizer.shape
    width = out.shape[1]
    size = width // heads
    props = out.shape[0] // seqs
    at = [slice(p * seqs, (p + 1) * seqs) for p in range(props)]
    row_scale = lax.rsqrt(squares[...] / model_width + epsilon)

    def projected(start, stop):
        total = functools.reduce(jnp.add, [part[:, start:stop].astype(f32) for part in parts])
        return total * row_scale

    queries = projected(0, width).astype(bf16).astype(f32)
    query_rows[...] = jnp.zeros_like(query_rows)
    for h in range(heads):
        query_rows[h, : props * seqs] = queries[:, h * size : (h + 1) * size]
    padded = query_rows.shape[1] // seqs
    for s in range(seqs):
        for h in range(heads):
            q = query_rows[h, pl.ds(s, padded, stride=seqs), :].astype(bf16)
            prior_rows[h, pl.ds(s, padded, stride=seqs), :] = jnp.dot(
                q, cell_low[s * heads + h], preferred_element_type=f32
            )
    key_rows[...] = projected(width, 2 * width).astype(bf16).astype(f32) * size**-0.5
    value_rows[...] = projected(2 * width, 3 * width).astype(bf16).astype(f32)
    outgate = projected(3 * width, 4 * width).astype(bf16).astype(f32)
    gates = projected(4 * width, 4 * width + 2 * heads) + projected(4 * width + 2 * heads, 4 * width + 4 * heads)
    log_in, running, keep = [], [], jnp.zeros((seqs, heads), f32)
    for p in range(props):
        log_in.append(gates[at[p], :heads])
        keep = keep + log_sigmoid(gates[at[p], heads:] + bias[...])
        running.append(keep)
    normer = norm[...]
    for t in range(props):
        q = queries[at[t]]
        log_d = [running[t] - running[u] + log_in[u] for u in range(t + 1)]
        log_p = running[t] + stabilizer[...]
        top = jnp.maximum(log_p, largest(log_d))
        prior = jnp.exp(log_p - top)
        numerator = over_lanes(prior, size) * jnp.concatenate([prior_rows[h, at[t]] for h in range(heads)], axis=1)
        denominator = prior * head_sums(q * normer, heads)
        for u in range(t + 1):
            score = head_sums(q * key_rows[at[u]], heads) * jnp.exp(log_d[u] - top)
            numerator = numerator + over_lanes(score, size) * value_rows[at[u]]
            denominator = denominator + score
        hidden = numerator / over_lanes(jnp.maximum(jnp.abs(denominator), jnp.exp(-top)), size)
        normed = hidden * over_lanes(lax.rsqrt(head_sums(hidden * hidden, heads) / size + epsilon), size) * gain[...]
        out[at[t]] = (jax.nn.sigmoid(outgate[at[t]]) * normed).astype(bf16)


def project_kernel(n, groups, width, gates, *refs):
    xs, mine, other, out = refs[:groups], refs[groups : groups + n], refs[groups + n : groups + 2 * n], refs[-1]
    rows = xs[0].shape[0]
    x = jnp.concatenate([ref[...] for ref in xs], axis=0)
    for i in range(5):
        take = slice(i * width, (i + 1) * width) if i < 4 else slice(5 * width, 5 * width + gates)
        w = jnp.concatenate([ref[:, take] for pair in zip(mine, other) for ref in pair], axis=0)
        part = jnp.dot(x, w, preferred_element_type=f32)
        high = part.astype(bf16)
        put = slice(i * width, i * width + (width if i < 4 else gates))
        for g in range(groups):
            out[g, :, put] = high[g * rows : (g + 1) * rows]
    low = (part - high.astype(f32)).astype(bf16)
    for g in range(groups):
        out[g, :, 4 * width + gates :] = low[g * rows : (g + 1) * rows]


def stack_kernel(start, *refs):
    *ins, out = refs
    for i, ref in enumerate(ins):
        out[i] = ref[:, start : start + out.shape[2]]


def mix_kernel(steps, ny, nz, groups, *refs):
    place, gated, out = refs[0], refs[1], refs[-1]
    at, lumps = 2, []
    for _ in steps:
        lumps.append((refs[at : at + ny], refs[at + ny : at + 2 * ny]))
        at += 2 * ny
    z, y, c, t = place[0], place[1], place[2], place[3]
    half = lumps[0][0][0].shape[1]
    unit = 2 * half
    per = nz // groups
    g = gated[...]
    for lump, (mine, other) in zip(steps, lumps):
        for i, s in enumerate(lump):
            owner = lax.rem(z - s + nz, nz)
            target = lax.rem(owner // per - t + groups, groups)
            start = lax.rem(owner, per) * ny
            w = jnp.concatenate([ref[i] for pair in zip(mine, other) for ref in pair], axis=0)
            part = lax.dot_general(g, w, (((1,), (1,)), ((), ())), preferred_element_type=f32)
            for sy in range(ny):
                block = start + lax.rem(y - sy + ny, ny)
                lanes = pl.ds(pl.multiple_of(block * unit, unit), unit)
                piece = part[:, sy * unit : (sy + 1) * unit]
                piece = jnp.where(c == 1, pltpu.roll(piece, half, 1), piece)
                out[target, :, lanes] = piece.astype(bf16)


def shards(
    tokens, norm_gain, w_query, w_key, w_value, w_outgate, w_gates, forget_bias, head_gain, w_mix,
    state_cell, state_norm, state_max, pend_keys, pend_values, pend_gates, accepted,
):
    seqs, props, model_width = tokens.shape
    rows = seqs * props
    heads = forget_bias.shape[0]
    size = state_cell.shape[-1]
    width = heads * size
    gates = 2 * heads
    nz, ny, groups = lax.axis_size("z"), lax.axis_size("y"), lax.axis_size("tp")
    place = jnp.stack([lax.axis_index(a) for a in ("z", "y", "c", "tp")]).astype(jnp.int32)

    def by_proposal(rank3):
        return jnp.swapaxes(rank3, 0, 1).reshape(rows, -1)

    depth = w_query.shape[0]
    packed = call(
        pack_kernel, array((depth, 5 * width + gates), bf16), [in_hbm] * 4,
        w_query, w_key, w_value, w_outgate, w_gates.reshape(depth, gates), w_mix,
        scratch=[pltpu.SemaphoreType.DMA((4,))], vmem=4,
    )
    mine = ring(packed, "z")
    other = [shift(chunk, "c", 1) for chunk in mine]

    scaled, squares = call(
        functools.partial(prep_kernel, nz, ny),
        (array((ny, rows, model_width // ny), bf16), array((rows, 1))), [in_smem],
        place, by_proposal(tokens), norm_gain[None], vmem=4,
    )
    xs = [scaled[0]] + [shift(scaled[s], "y", s) for s in range(1, ny)]

    cell_new, cell_low, norm_new, new_max = call(
        fold_kernel,
        (
            array((seqs * heads, size, size)), array((seqs * heads, size, size), bf16),
            array((seqs, width)), array((seqs, heads)),
        ),
        [],
        state_cell.reshape(seqs * heads, size, size), state_norm.reshape(seqs, width), state_max,
        by_proposal(pend_keys), by_proposal(pend_values),
        by_proposal(pend_gates[:, :, 0]), by_proposal(pend_gates[:, :, 1]), forget_bias[None], accepted[:, None],
        scratch=[pltpu.VMEM((heads, 8 * seqs, size), f32)] * 2, vmem=12,
    )

    steps = ((0, 1, nz - 1, 2, nz - 2), tuple(range(3, nz - 2)))
    lumps = []
    for step in steps:
        stacked = call(
            functools.partial(stack_kernel, 4 * width), array((len(step), depth, width), bf16), [],
            *[mine[s] for s in step], vmem=6,
        )
        lump = direct(stacked, "y")
        lumps += [*lump, *[shift(piece, "c", 1) for piece in lump]]

    parts = call(
        functools.partial(project_kernel, nz, ny, width, gates), array((ny, rows, 4 * width + 2 * gates), bf16), [],
        *xs, *mine, *other, flops=2 * ny * rows * nz * 2 * depth * 4 * width, vmem=24,
    )
    home = [parts[0]] + [shift(parts[s], "y", -s) for s in range(1, ny)]
    gated = call(
        functools.partial(read_kernel, model_width), array((rows, width), bf16), [],
        *home, squares, cell_low, norm_new, new_max, forget_bias[None], head_gain[None],
        scratch=[pltpu.VMEM((heads, 8 * seqs, size), f32)] * 2 + [pltpu.VMEM((rows, width), f32)] * 2, vmem=12,
    )

    columns = nz * ny * 2 * depth
    sums = call(
        functools.partial(mix_kernel, steps, ny, nz, groups), array((groups, rows, columns // groups), bf16), [in_smem],
        place, gated, *lumps, flops=2 * rows * width * columns, vmem=16,
    )
    arrived = [sums[0]] + [shift(sums[s], "tp", s) for s in range(1, groups)]
    mixed = functools.reduce(jnp.add, [part.astype(f32) for part in arrived]).astype(bf16)
    return (
        jnp.swapaxes(mixed.reshape(props, seqs, -1), 0, 1),
        cell_new.reshape(state_cell.shape), norm_new.reshape(state_norm.shape), new_max,
    )


def solution(mesh):
    grid = Mesh(mesh.devices.reshape(8, 4, 2, mesh.shape["tp"]), ("z", "y", "c", "tp"))
    kv = ("z", "y", "c")
    return jax.shard_map(
        shards,
        mesh=grid,
        in_specs=(
            P(kv, None, None), P(), P(kv, "tp"), P(kv, "tp"), P(kv, "tp"), P(kv, "tp"), P(kv, None, "tp"),
            P("tp"), P("tp"), P("tp", kv), P(kv, "tp", None, None), P(kv, "tp", None), P(kv, "tp"),
            P(kv, None, "tp"), P(kv, None, "tp"), P(kv, None, None, "tp"), P(kv),
        ),
        out_specs=(P(kv, None, "tp"), P(kv, "tp", None, None), P(kv, "tp", None), P(kv, "tp")),
        check_vma=False,
    )
```

time: 125 us -> 112 us (0.90)
  starting transfers between devices: 69.9 us -> 55.9 us
  waiting for transfers between devices: 18.6 us -> 28.2 us
  matrix products: 5.73 us -> 0 us
  other arithmetic: 6.16 us -> 0.77 us
  Pallas kernels: 5.39 us -> 10.5 us
  local copies, waits for them, and re-layouts: 16.9 us -> 14.9 us
    ppermute x43 -> x38, starting transfers between devices: 69.2 us -> 55.9 us  [shift(): return lax.ppermute(array, axis, [(j, (j + by) % n) for j in range(n)])]
    ppermute x43 -> x38, waiting for transfers between devices: 18.6 us -> 28.2 us  [shift(): return lax.ppermute(array, axis, [(j, (j + by) % n) for j in range(n)])]
    dot_general x5 -> x0, matrix products: 5.73 us -> none  [the longest x1 3.7 us: fold_pending(): jnp.einsum('sphd,sphe->shde', weighted_keys, value_rows, precision=highest)]
    pallas_call x4 -> x8, Pallas kernels: 5.39 us -> 10.5 us  [call(): pl.pallas_call(kernel, out_shape=out_shape, in_specs=specs + [in_vmem] *...]
    another operation x4 -> x1, other arithmetic: 3.04 us -> 0.08 us  [shards(): jnp.stack([lax.axis_index(a) for a in ('z', 'y', 'c', 'tp')])]
    unnamed x63 -> x65, local copies, waits for them, and re-layouts: 13.8 us -> 13.1 us
  transfers between devices with their start and end apart: 44 -> 38, of which waited for: 7 -> 10; matrix products, arithmetic and copies ran while one was open for 15% -> 3% of each run, Pallas kernels for 3% -> 7%
where the time goes in v2:
time: 112 us; the launch traced here: 111 us
  starting transfers between devices  55.9 us (50%)
  waiting for transfers between devices  28.2 us (25%)
  local copies, waits for them, and re-layouts  14.9 us (13%)
  Pallas kernels  10.5 us (9%)
    ppermute x38, starting transfers between devices, shift(): return lax.ppermute(array, axis, [(j, (j + by) % n) for j in range(n)])  55.9 us
    ppermute x38, waiting for transfers between devices, shift(): return lax.ppermute(array, axis, [(j, (j + by) % n) for j in range(n)])  28.2 us
    unnamed x65, local copies, waits for them, and re-layouts  13.1 us
    pallas_call x8, Pallas kernels, call(): pl.pallas_call(kernel, out_shape=out_shape, in_specs=specs + [in_vmem] *...  10.5 us
  transfers between devices with their start and end apart: 38, of which 10 were waited for; matrix products, arithmetic and copies ran while one was open for 3% of the time, Pallas kernels for 7%

profile of v2, /device:TPU:1, one launch (start us, length us, event | category | flops | bytes accessed | tf_op | source)
XLA Modules:
  0.0 111.3 jit_solution(8176004674951024859)
XLA Ops:
  5.9 2.5 %collective-permute-start.3 = (bf16[64,2568]{1,0:T(8,128)(2,1)S(1)}, bf16[64,2568]{1,0:T(8,128)(2,1)S(1)}, u32[]{:S(2)}, u32[]{:S(2)}) collective-permute-start(bf16[64,2568]{1,0:T(8,128)(2,1)S(1)} %shard_map.193.refs_4_.refs_0_), channel_id=1, source_target_pairs={{0,32},{32,64},{64,96},{96,128},{128,160},{160,192},{192,224},{224... | collective-permute-start | bytes 986120 | tf_op jit(solution)/shard_map/ppermute | solution.py:22
  8.4 4.0 %collective-permute-start.7 = (bf16[64,2568]{1,0:T(8,128)(2,1)S(1)}, bf16[64,2568]{1,0:T(8,128)(2,1)S(1)}, u32[]{:S(2)}, u32[]{:S(2)}) collective-permute-start(bf16[64,2568]{1,0:T(8,128)(2,1)S(1)} %shard_map.193.refs_4_.refs_0_), channel_id=1, source_target_pairs={{0,224},{32,0},{64,32},{96,64},{128,96},{160,128},{192,160},{224,1... | collective-permute-start | bytes 986120 | tf_op jit(solution)/shard_map/ppermute | solution.py:22
  15.1 5.0 %collective-permute-done.3.refs_5_.refs_1_ = bf16[64,2568]{1,0:T(8,128)(2,1)S(1)} collective-permute-done((bf16[64,2568]{1,0:T(8,128)(2,1)S(1)}, bf16[64,2568]{1,0:T(8,128)(2,1)S(1)}, u32[]{:S(2)}, u32[]{:S(2)}) %collective-permute-start.3) | collective-permute-done | bytes 328736 | tf_op jit(solution)/shard_map/ppermute | solution.py:22
  20.2 1.4 %collective-permute-start = (bf16[48,1024]{1,0:T(8,128)(2,1)S(1)}, bf16[48,1024]{1,0:T(8,128)(2,1)S(1)}, u32[]{:S(2)}, u32[]{:S(2)}) collective-permute-start(bf16[48,1024]{1,0:T(8,128)(2,1)S(1)} %get-tuple-element.33), channel_id=1, source_target_pairs={{0,8},{8,16},{16,24},{24,0},{1,9},{9,17},{17,25},{25,1},{2,10},{10... | collective-permute-start | bytes 294920 | tf_op jit(solution)/shard_map/ppermute | solution.py:22
  21.6 2.6 %collective-permute-start.1 = (bf16[48,1024]{1,0:T(8,128)(2,1)S(1)}, bf16[48,1024]{1,0:T(8,128)(2,1)S(1)}, u32[]{:S(2)}, u32[]{:S(2)}) collective-permute-start(bf16[48,1024]{1,0:T(8,128)(2,1)S(1)} %get-tuple-element.32), channel_id=1, source_target_pairs={{0,16},{8,24},{16,0},{24,8},{1,17},{9,25},{17,1},{25,9},{2,18},{10... | collective-permute-start | bytes 294920 | tf_op jit(solution)/shard_map/ppermute | solution.py:22
  24.2 1.1 collective-permute-start.2
  25.2 2.7 %collective-permute-start.8 = (bf16[64,2568]{1,0:T(8,128)(2,1)S(1)}, bf16[64,2568]{1,0:T(8,128)(2,1)S(1)}, u32[]{:S(2)}, u32[]{:S(2)}) collective-permute-start(bf16[64,2568]{1,0:T(8,128)(2,1)S(1)} %collective-permute-done.7.refs_11_.refs_2_), channel_id=1, source_target_pairs={{0,224},{32,0},{64,32},{96,64},{128,96},{160,128},{192,160},{224,1... | collective-permute-start | bytes 986120 | tf_op jit(solution)/shard_map/ppermute | solution.py:22
  27.9 1.8 %collective-permute-done.4.refs_6_.refs_3_ = bf16[64,2568]{1,0:T(8,128)(2,1)S(1)} collective-permute-done((bf16[64,2568]{1,0:T(8,128)(2,1)S(1)}, bf16[64,2568]{1,0:T(8,128)(2,1)S(1)}, u32[]{:S(2)}, u32[]{:S(2)}) %collective-permute-start.4) | collective-permute-done | bytes 328736 | tf_op jit(solution)/shard_map/ppermute | solution.py:22
  29.7 2.1 %collective-permute-start.10 = (bf16[64,2568]{1,0:T(8,128)(2,1)S(1)}, bf16[64,2568]{1,0:T(8,128)(2,1)S(1)}, u32[]{:S(2)}, u32[]{:S(2)}) collective-permute-start(bf16[64,2568]{1,0:T(8,128)(2,1)S(1)} %shard_map.193.refs_4_.refs_0_), channel_id=1, source_target_pairs={{0,4},{4,0},{1,5},{5,1},{2,6},{6,2},{3,7},{7,3},{8,12},{12,8},{9,1... | collective-permute-start | bytes 986120 | tf_op jit(solution)/shard_map/ppermute | solution.py:22
  33.0 3.4 %collective-permute-start.9 = (bf16[64,2568]{1,0:T(8,128)(2,1)S(1)}, bf16[64,2568]{1,0:T(8,128)(2,1)S(1)}, u32[]{:S(2)}, u32[]{:S(2)}) collective-permute-start(bf16[64,2568]{1,0:T(8,128)(2,1)S(1)} %collective-permute-done.8.refs_10_.refs_4_), channel_id=1, source_target_pairs={{0,224},{32,0},{64,32},{96,64},{128,96},{160,128},{192,160},{224,1... | collective-permute-start | bytes 986120 | tf_op jit(solution)/shard_map/ppermute | solution.py:22
  36.4 2.1 %collective-permute-done.5.refs_7_.refs_0_ = bf16[64,2568]{1,0:T(8,128)(2,1)S(1)} collective-permute-done((bf16[64,2568]{1,0:T(8,128)(2,1)S(1)}, bf16[64,2568]{1,0:T(8,128)(2,1)S(1)}, u32[]{:S(2)}, u32[]{:S(2)}) %collective-permute-start.5) | collective-permute-done | bytes 328736 | tf_op jit(solution)/shard_map/ppermute | solution.py:22
  38.5 1.4 %collective-permute-start.21 = (bf16[5,64,512]{2,1,0:T(8,128)(2,1)S(1)}, bf16[5,64,512]{2,1,0:T(8,128)(2,1)S(1)}, u32[]{:S(2)}, u32[]{:S(2)}) collective-permute-start(bf16[5,64,512]{2,1,0:T(8,128)(2,1)S(1)} %shard_map.197.refs_2_), channel_id=1, source_target_pairs={{0,8},{8,16},{16,24},{24,0},{1,9},{9,17},{17,25},{25,1},{2,10},{10... | collective-permute-start | bytes 983048 | tf_op jit(solution)/shard_map/ppermute | solution.py:22
  39.9 2.6 %collective-permute-start.22 = (bf16[5,64,512]{2,1,0:T(8,128)(2,1)S(1)}, bf16[5,64,512]{2,1,0:T(8,128)(2,1)S(1)}, u32[]{:S(2)}, u32[]{:S(2)}) collective-permute-start(bf16[5,64,512]{2,1,0:T(8,128)(2,1)S(1)} %shard_map.197.refs_2_), channel_id=1, source_target_pairs={{0,16},{8,24},{16,0},{24,8},{1,17},{9,25},{17,1},{25,9},{2,18},{10... | collective-permute-start | bytes 983048 | tf_op jit(solution)/shard_map/ppermute | solution.py:22
  42.5 3.5 %collective-permute-start.12 = (bf16[64,2568]{1,0:T(8,128)(2,1)S(1)}, bf16[64,2568]{1,0:T(8,128)(2,1)S(1)}, u32[]{:S(2)}, u32[]{:S(2)}) collective-permute-start(bf16[64,2568]{1,0:T(8,128)(2,1)S(1)} %collective-permute-done.4.refs_6_.refs_3_), channel_id=1, source_target_pairs={{0,4},{4,0},{1,5},{5,1},{2,6},{6,2},{3,7},{7,3},{8,12},{12,8},{9,1... | collective-permute-start | bytes 986120 | tf_op jit(solution)/shard_map/ppermute | solution.py:22
  46.2 6.0 %collective-permute-start.16 = (bf16[64,2568]{1,0:T(8,128)(2,1)S(1)}, bf16[64,2568]{1,0:T(8,128)(2,1)S(1)}, u32[]{:S(2)}, u32[]{:S(2)}) collective-permute-start(bf16[64,2568]{1,0:T(8,128)(2,1)S(1)} %collective-permute-done.8.refs_10_.refs_4_), channel_id=1, source_target_pairs={{0,4},{4,0},{1,5},{5,1},{2,6},{6,2},{3,7},{7,3},{8,12},{12,8},{9,1... | collective-permute-start | bytes 986120 | tf_op jit(solution)/shard_map/ppermute | solution.py:22
  52.2 2.1 %collective-permute-done.22.refs_4_ = bf16[5,64,512]{2,1,0:T(8,128)(2,1)S(1)} collective-permute-done((bf16[5,64,512]{2,1,0:T(8,128)(2,1)S(1)}, bf16[5,64,512]{2,1,0:T(8,128)(2,1)S(1)}, u32[]{:S(2)}, u32[]{:S(2)}) %collective-permute-start.22) | collective-permute-done | bytes 327712 | tf_op jit(solution)/shard_map/ppermute | solution.py:22
  54.3 3.8 %collective-permute-start.13 = (bf16[64,2568]{1,0:T(8,128)(2,1)S(1)}, bf16[64,2568]{1,0:T(8,128)(2,1)S(1)}, u32[]{:S(2)}, u32[]{:S(2)}) collective-permute-start(bf16[64,2568]{1,0:T(8,128)(2,1)S(1)} %collective-permute-done.5.refs_7_.refs_0_), channel_id=1, source_target_pairs={{0,4},{4,0},{1,5},{5,1},{2,6},{6,2},{3,7},{7,3},{8,12},{12,8},{9,1... | collective-permute-start | bytes 986120 | tf_op jit(solution)/shard_map/ppermute | solution.py:22
  60.4 1.3 %collective-permute-start.28 = (bf16[3,64,512]{2,1,0:T(8,128)(2,1)}, bf16[3,64,512]{2,1,0:T(8,128)(2,1)}, u32[]{:S(2)}, u32[]{:S(2)}) collective-permute-start(bf16[3,64,512]{2,1,0:T(8,128)(2,1)} %shard_map.198.refs_10_), channel_id=1, source_target_pairs={{0,8},{8,16},{16,24},{24,0},{1,9},{9,17},{17,25},{25,1},{2,10},{10... | collective-permute-start | bytes 589832 | tf_op jit(solution)/shard_map/ppermute | solution.py:22
  61.8 1.2 %shard_map.194 = bf16[4,48,2064]{2,1,0:T(8,128)(2,1)S(1)} custom-call(bf16[48,1024]{1,0:T(8,128)(2,1)S(1)} %get-tuple-element.34.refs_0_, bf16[48,1024]{1,0:T(8,128)(2,1)S(1)} %collective-permute-done.refs_1_, bf16[48,1024]{1,0:T(8,128)(2,1)S(1)} %collective-permute-done.1.refs_2_, bf16[48,1024]{1,0:T(8,128)(2,1)S(1)} %collective-permute-done.2.refs_3_, ...), custom_call_target="tpu_custom_call" | custom-call | flops 805306368 | bytes 6445056 | tf_op jit(solution)/shard_map/pallas_call | solution.py:45
  63.0 5.0 %collective-permute-done.23.refs_5_ = bf16[5,64,512]{2,1,0:T(8,128)(2,1)} collective-permute-done((bf16[5,64,512]{2,1,0:T(8,128)(2,1)S(1)}, bf16[5,64,512]{2,1,0:T(8,128)(2,1)}, u32[]{:S(2)}, u32[]{:S(2)}) %collective-permute-start.23) | collective-permute-done | bytes 327712 | tf_op jit(solution)/shard_map/ppermute | solution.py:22
  71.0 2.3 %collective-permute-start.19 = (bf16[48,2064]{1,0:T(8,128)(2,1)S(1)}, bf16[48,2064]{1,0:T(8,128)(2,1)S(1)}, u32[]{:S(2)}, u32[]{:S(2)}) collective-permute-start(bf16[48,2064]{1,0:T(8,128)(2,1)S(1)} %get-tuple-element.25), channel_id=1, source_target_pairs={{0,16},{8,24},{16,0},{24,8},{1,17},{9,25},{17,1},{25,9},{2,18},{10... | collective-permute-start | bytes 594440 | tf_op jit(solution)/shard_map/ppermute | solution.py:22
  74.1 2.7 %collective-permute-start.30 = (bf16[3,64,512]{2,1,0:T(8,128)(2,1)}, bf16[3,64,512]{2,1,0:T(8,128)(2,1)}, u32[]{:S(2)}, u32[]{:S(2)}) collective-permute-start(bf16[3,64,512]{2,1,0:T(8,128)(2,1)} %shard_map.198.refs_10_), channel_id=1, source_target_pairs={{0,24},{8,0},{16,8},{24,16},{1,25},{9,1},{17,9},{25,17},{2,26},{10... | collective-permute-start | bytes 589832 | tf_op jit(solution)/shard_map/ppermute | solution.py:22
  76.8 2.1 %collective-permute-start.27 = (bf16[5,64,512]{2,1,0:T(8,128)(2,1)}, bf16[5,64,512]{2,1,0:T(8,128)(2,1)S(1)}, u32[]{:S(2)}, u32[]{:S(2)}) collective-permute-start(bf16[5,64,512]{2,1,0:T(8,128)(2,1)} %collective-permute-done.23.refs_5_), channel_id=1, source_target_pairs={{0,4},{4,0},{1,5},{5,1},{2,6},{6,2},{3,7},{7,3},{8,12},{12,8},{9,1... | collective-permute-start | bytes 983048 | tf_op jit(solution)/shard_map/ppermute | solution.py:22
  78.8 9.1 %collective-permute-done.30.refs_13_ = bf16[3,64,512]{2,1,0:T(8,128)(2,1)} collective-permute-done((bf16[3,64,512]{2,1,0:T(8,128)(2,1)}, bf16[3,64,512]{2,1,0:T(8,128)(2,1)}, u32[]{:S(2)}, u32[]{:S(2)}) %collective-permute-start.30) | collective-permute-done | bytes 196640 | tf_op jit(solution)/shard_map/ppermute | solution.py:22
  87.9 1.5 %collective-permute-start.31 = (bf16[3,64,512]{2,1,0:T(8,128)(2,1)}, bf16[3,64,512]{2,1,0:T(8,128)(2,1)}, u32[]{:S(2)}, u32[]{:S(2)}) collective-permute-start(bf16[3,64,512]{2,1,0:T(8,128)(2,1)} %shard_map.198.refs_10_), channel_id=1, source_target_pairs={{0,4},{4,0},{1,5},{5,1},{2,6},{6,2},{3,7},{7,3},{8,12},{12,8},{9,1... | collective-permute-start | bytes 589832 | tf_op jit(solution)/shard_map/ppermute | solution.py:22
  94.6 2.2 %shard_map.195 = (f32[32,128,128]{2,1,0:T(8,128)}, bf16[32,128,128]{2,1,0:T(8,128)(2,1)S(1)}, f32[8,512]{1,0:T(8,128)S(1)}, f32[8,4]{1,0:T(8,128)S(1)}) custom-call(f32[32,128,128]{2,1,0:T(8,128)S(1)} %bitcast.66, f32[8,512]{1,0:T(8,128)S(1)} %bitcast.71, f32[8,4]{1,0:T(8,128)S(1)} %copy.33.stabilizer, bf16[48,512]{1,0:T(8,128)(2,1)S(1)} %bitcast.72, ...), custom_call_target="tpu_custom_call" | custom-call | flops 10751584 | bytes 5375792 | tf_op jit(solution)/shard_map/pallas_call | solution.py:45
  96.8 2.4 %shard_map.196.refs_1_ = bf16[48,512]{1,0:T(8,128)(2,1)S(1)} custom-call(bf16[48,2064]{1,0:T(8,128)(2,1)S(1)} %get-tuple-element.27.refs_0_, bf16[48,2064]{1,0:T(8,128)(2,1)S(1)} %collective-permute-done.18.refs_1_, bf16[48,2064]{1,0:T(8,128)(2,1)S(1)} %copy-done.13, bf16[48,2064]{1,0:T(8,128)(2,1)S(1)} %copy-done.15, f32[48,1]{1,0:T(8,128)S(1)} %copy-done.23, ...), custom_call_target="tpu_custom_call" | custom-call | flops 3818144 | bytes 1909072 | tf_op jit(solution)/shard_map/pallas_call | solution.py:45
  99.3 3.0 %shard_map.199 = bf16[4,48,1024]{2,1,0:T(8,128)(2,1)S(1)} custom-call(s32[4]{0:T(128)S(1)} %copy-done.26, bf16[48,512]{1,0:T(8,128)(2,1)S(1)} %shard_map.196.refs_1_, bf16[5,64,512]{2,1,0:T(8,128)(2,1)S(1)} %shard_map.197.refs_2_, bf16[5,64,512]{2,1,0:T(8,128)(2,1)S(1)} %copy-done.3, bf16[5,64,512]{2,1,0:T(8,128)(2,1)S(1)} %copy-done.5, ...), custom_call_target="tpu_custom_call" | custom-call | flops 201326592 | bytes 4636688 | tf_op jit(solution)/shard_map/pallas_call | solution.py:45
  102.4 1.3 %collective-permute-start.35 = (bf16[48,1024]{1,0:T(8,128)(2,1)S(1)}, bf16[48,1024]{1,0:T(8,128)(2,1)S(1)}, u32[]{:S(2)}, u32[]{:S(2)}) collective-permute-start(bf16[48,1024]{1,0:T(8,128)(2,1)S(1)} %get-tuple-element.28), channel_id=1, source_target_pairs={{0,1},{1,2},{2,3},{3,0},{4,5},{5,6},{6,7},{7,4},{8,9},{9,10},{10,1... | collective-permute-start | bytes 294920 | tf_op jit(solution)/shard_map/ppermute | solution.py:22
  103.6 2.5 %collective-permute-start.36 = (bf16[48,1024]{1,0:T(8,128)(2,1)S(1)}, bf16[48,1024]{1,0:T(8,128)(2,1)S(1)}, u32[]{:S(2)}, u32[]{:S(2)}) collective-permute-start(bf16[48,1024]{1,0:T(8,128)(2,1)S(1)} %get-tuple-element.30), channel_id=1, source_target_pairs={{0,2},{1,3},{2,0},{3,1},{4,6},{5,7},{6,4},{7,5},{8,10},{9,11},{10,... | collective-permute-start | bytes 294920 | tf_op jit(solution)/shard_map/ppermute | solution.py:22
  106.1 1.1 %collective-permute-start.37 = (bf16[48,1024]{1,0:T(8,128)(2,1)S(1)}, bf16[48,1024]{1,0:T(8,128)(2,1)S(1)}, u32[]{:S(2)}, u32[]{:S(2)}) collective-permute-start(bf16[48,1024]{1,0:T(8,128)(2,1)S(1)} %get-tuple-element.29), channel_id=1, source_target_pairs={{0,3},{1,0},{2,1},{3,2},{4,7},{5,4},{6,5},{7,6},{8,11},{9,8},{10,9... | collective-permute-start | bytes 294920 | tf_op jit(solution)/shard_map/ppermute | solution.py:22
  108.5 2.1 %collective-permute-done.36 = bf16[48,1024]{1,0:T(8,128)(2,1)S(1)} collective-permute-done((bf16[48,1024]{1,0:T(8,128)(2,1)S(1)}, bf16[48,1024]{1,0:T(8,128)(2,1)S(1)}, u32[]{:S(2)}, u32[]{:S(2)}) %collective-permute-start.36) | collective-permute-done | bytes 98336 | tf_op jit(solution)/shard_map/ppermute | solution.py:22
  (127 shorter events, 22.4 us)
Async XLA Ops:
  5.9 14.2 %collective-permute-start.3 = (bf16[64,2568]{1,0:T(8,128)(2,1)S(1)}, bf16[64,2568]{1,0:T(8,128)(2,1)S(1)}, u32[]{:S(2)}, u32[]{:S(2)}) collective-permute-start(bf16[64,2568]{1,0:T(8,128)(2,1)S(1)} %shard_map.193.refs_4_.refs_0_), channel_id=1, source_target_pairs={{0,32},{32,64},{64,96},{96,128},{128,160},{160,192},{192,224},{224... | collective-permute-start | bytes 986120 | tf_op jit(solution)/shard_map/ppermute | solution.py:22
  8.4 16.8 %collective-permute-start.7 = (bf16[64,2568]{1,0:T(8,128)(2,1)S(1)}, bf16[64,2568]{1,0:T(8,128)(2,1)S(1)}, u32[]{:S(2)}, u32[]{:S(2)}) collective-permute-start(bf16[64,2568]{1,0:T(8,128)(2,1)S(1)} %shard_map.193.refs_4_.refs_0_), channel_id=1, source_target_pairs={{0,224},{32,0},{64,32},{96,64},{128,96},{160,128},{192,160},{224,1... | collective-permute-start | bytes 986120 | tf_op jit(solution)/shard_map/ppermute | solution.py:22
  20.1 9.6 %collective-permute-start.4 = (bf16[64,2568]{1,0:T(8,128)(2,1)S(1)}, bf16[64,2568]{1,0:T(8,128)(2,1)S(1)}, u32[]{:S(2)}, u32[]{:S(2)}) collective-permute-start(bf16[64,2568]{1,0:T(8,128)(2,1)S(1)} %collective-permute-done.3.refs_5_.refs_1_), channel_id=1, source_target_pairs={{0,32},{32,64},{64,96},{96,128},{128,160},{160,192},{192,224},{224... | collective-permute-start | bytes 986120 | tf_op jit(solution)/shard_map/ppermute | solution.py:22
  20.2 9.6 %collective-permute-start = (bf16[48,1024]{1,0:T(8,128)(2,1)S(1)}, bf16[48,1024]{1,0:T(8,128)(2,1)S(1)}, u32[]{:S(2)}, u32[]{:S(2)}) collective-permute-start(bf16[48,1024]{1,0:T(8,128)(2,1)S(1)} %get-tuple-element.33), channel_id=1, source_target_pairs={{0,8},{8,16},{16,24},{24,0},{1,9},{9,17},{17,25},{25,1},{2,10},{10... | collective-permute-start | bytes 294920 | tf_op jit(solution)/shard_map/ppermute | solution.py:22
  21.6 10.3 %collective-permute-start.1 = (bf16[48,1024]{1,0:T(8,128)(2,1)S(1)}, bf16[48,1024]{1,0:T(8,128)(2,1)S(1)}, u32[]{:S(2)}, u32[]{:S(2)}) collective-permute-start(bf16[48,1024]{1,0:T(8,128)(2,1)S(1)} %get-tuple-element.32), channel_id=1, source_target_pairs={{0,16},{8,24},{16,0},{24,8},{1,17},{9,25},{17,1},{25,9},{2,18},{10... | collective-permute-start | bytes 294920 | tf_op jit(solution)/shard_map/ppermute | solution.py:22
  24.2 7.8 %collective-permute-start.2 = (bf16[48,1024]{1,0:T(8,128)(2,1)S(1)}, bf16[48,1024]{1,0:T(8,128)(2,1)S(1)}, u32[]{:S(2)}, u32[]{:S(2)}) collective-permute-start(bf16[48,1024]{1,0:T(8,128)(2,1)S(1)} %get-tuple-element.31), channel_id=1, source_target_pairs={{0,24},{8,0},{16,8},{24,16},{1,25},{9,1},{17,9},{25,17},{2,26},{10... | collective-permute-start | bytes 294920 | tf_op jit(solution)/shard_map/ppermute | solution.py:22
  25.2 7.7 %collective-permute-start.8 = (bf16[64,2568]{1,0:T(8,128)(2,1)S(1)}, bf16[64,2568]{1,0:T(8,128)(2,1)S(1)}, u32[]{:S(2)}, u32[]{:S(2)}) collective-permute-start(bf16[64,2568]{1,0:T(8,128)(2,1)S(1)} %collective-permute-done.7.refs_11_.refs_2_), channel_id=1, source_target_pairs={{0,224},{32,0},{64,32},{96,64},{128,96},{160,128},{192,160},{224,1... | collective-permute-start | bytes 986120 | tf_op jit(solution)/shard_map/ppermute | solution.py:22
  29.7 8.7 %collective-permute-start.5 = (bf16[64,2568]{1,0:T(8,128)(2,1)S(1)}, bf16[64,2568]{1,0:T(8,128)(2,1)S(1)}, u32[]{:S(2)}, u32[]{:S(2)}) collective-permute-start(bf16[64,2568]{1,0:T(8,128)(2,1)S(1)} %collective-permute-done.4.refs_6_.refs_3_), channel_id=1, source_target_pairs={{0,32},{32,64},{64,96},{96,128},{128,160},{160,192},{192,224},{224... | collective-permute-start | bytes 986120 | tf_op jit(solution)/shard_map/ppermute | solution.py:22
  29.7 8.8 %collective-permute-start.10 = (bf16[64,2568]{1,0:T(8,128)(2,1)S(1)}, bf16[64,2568]{1,0:T(8,128)(2,1)S(1)}, u32[]{:S(2)}, u32[]{:S(2)}) collective-permute-start(bf16[64,2568]{1,0:T(8,128)(2,1)S(1)} %shard_map.193.refs_4_.refs_0_), channel_id=1, source_target_pairs={{0,4},{4,0},{1,5},{5,1},{2,6},{6,2},{3,7},{7,3},{8,12},{12,8},{9,1... | collective-permute-start | bytes 986120 | tf_op jit(solution)/shard_map/ppermute | solution.py:22
  31.8 8.0 %collective-permute-start.11 = (bf16[64,2568]{1,0:T(8,128)(2,1)S(1)}, bf16[64,2568]{1,0:T(8,128)(2,1)S(1)}, u32[]{:S(2)}, u32[]{:S(2)}) collective-permute-start(bf16[64,2568]{1,0:T(8,128)(2,1)S(1)} %collective-permute-done.3.refs_5_.refs_1_), channel_id=1, source_target_pairs={{0,4},{4,0},{1,5},{5,1},{2,6},{6,2},{3,7},{7,3},{8,12},{12,8},{9,1... | collective-permute-start | bytes 986120 | tf_op jit(solution)/shard_map/ppermute | solution.py:22
  31.9 10.5 %collective-permute-start.17 = (bf16[64,2568]{1,0:T(8,128)(2,1)S(1)}, bf16[64,2568]{1,0:T(8,128)(2,1)S(1)}, u32[]{:S(2)}, u32[]{:S(2)}) collective-permute-start(bf16[64,2568]{1,0:T(8,128)(2,1)S(1)} %collective-permute-done.7.refs_11_.refs_2_), channel_id=1, source_target_pairs={{0,4},{4,0},{1,5},{5,1},{2,6},{6,2},{3,7},{7,3},{8,12},{12,8},{9,1... | collective-permute-start | bytes 986120 | tf_op jit(solution)/shard_map/ppermute | solution.py:22
  33.0 25.2 %collective-permute-start.9 = (bf16[64,2568]{1,0:T(8,128)(2,1)S(1)}, bf16[64,2568]{1,0:T(8,128)(2,1)S(1)}, u32[]{:S(2)}, u32[]{:S(2)}) collective-permute-start(bf16[64,2568]{1,0:T(8,128)(2,1)S(1)} %collective-permute-done.8.refs_10_.refs_4_), channel_id=1, source_target_pairs={{0,224},{32,0},{64,32},{96,64},{128,96},{160,128},{192,160},{224,1... | collective-permute-start | bytes 986120 | tf_op jit(solution)/shard_map/ppermute | solution.py:22
  38.4 19.8 %collective-permute-start.6 = (bf16[64,2568]{1,0:T(8,128)(2,1)S(1)}, bf16[64,2568]{1,0:T(8,128)(2,1)S(1)}, u32[]{:S(2)}, u32[]{:S(2)}) collective-permute-start(bf16[64,2568]{1,0:T(8,128)(2,1)S(1)} %collective-permute-done.5.refs_7_.refs_0_), channel_id=1, source_target_pairs={{0,32},{32,64},{64,96},{96,128},{128,160},{160,192},{192,224},{224... | collective-permute-start | bytes 986120 | tf_op jit(solution)/shard_map/ppermute | solution.py:22
  38.5 7.7 %collective-permute-start.21 = (bf16[5,64,512]{2,1,0:T(8,128)(2,1)S(1)}, bf16[5,64,512]{2,1,0:T(8,128)(2,1)S(1)}, u32[]{:S(2)}, u32[]{:S(2)}) collective-permute-start(bf16[5,64,512]{2,1,0:T(8,128)(2,1)S(1)} %shard_map.197.refs_2_), channel_id=1, source_target_pairs={{0,8},{8,16},{16,24},{24,0},{1,9},{9,17},{17,25},{25,1},{2,10},{10... | collective-permute-start | bytes 983048 | tf_op jit(solution)/shard_map/ppermute | solution.py:22
  39.9 14.5 %collective-permute-start.22 = (bf16[5,64,512]{2,1,0:T(8,128)(2,1)S(1)}, bf16[5,64,512]{2,1,0:T(8,128)(2,1)S(1)}, u32[]{:S(2)}, u32[]{:S(2)}) collective-permute-start(bf16[5,64,512]{2,1,0:T(8,128)(2,1)S(1)} %shard_map.197.refs_2_), channel_id=1, source_target_pairs={{0,16},{8,24},{16,0},{24,8},{1,17},{9,25},{17,1},{25,9},{2,18},{10... | collective-permute-start | bytes 983048 | tf_op jit(solution)/shard_map/ppermute | solution.py:22
  42.5 16.2 %collective-permute-start.12 = (bf16[64,2568]{1,0:T(8,128)(2,1)S(1)}, bf16[64,2568]{1,0:T(8,128)(2,1)S(1)}, u32[]{:S(2)}, u32[]{:S(2)}) collective-permute-start(bf16[64,2568]{1,0:T(8,128)(2,1)S(1)} %collective-permute-done.4.refs_6_.refs_3_), channel_id=1, source_target_pairs={{0,4},{4,0},{1,5},{5,1},{2,6},{6,2},{3,7},{7,3},{8,12},{12,8},{9,1... | collective-permute-start | bytes 986120 | tf_op jit(solution)/shard_map/ppermute | solution.py:22
  46.2 13.2 %collective-permute-start.16 = (bf16[64,2568]{1,0:T(8,128)(2,1)S(1)}, bf16[64,2568]{1,0:T(8,128)(2,1)S(1)}, u32[]{:S(2)}, u32[]{:S(2)}) collective-permute-start(bf16[64,2568]{1,0:T(8,128)(2,1)S(1)} %collective-permute-done.8.refs_10_.refs_4_), channel_id=1, source_target_pairs={{0,4},{4,0},{1,5},{5,1},{2,6},{6,2},{3,7},{7,3},{8,12},{12,8},{9,1... | collective-permute-start | bytes 986120 | tf_op jit(solution)/shard_map/ppermute | solution.py:22
  58.7 9.3 %collective-permute-start.23 = (bf16[5,64,512]{2,1,0:T(8,128)(2,1)S(1)}, bf16[5,64,512]{2,1,0:T(8,128)(2,1)}, u32[]{:S(2)}, u32[]{:S(2)}) collective-permute-start(bf16[5,64,512]{2,1,0:T(8,128)(2,1)S(1)} %shard_map.197.refs_2_), channel_id=1, source_target_pairs={{0,24},{8,0},{16,8},{24,16},{1,25},{9,1},{17,9},{25,17},{2,26},{10... | collective-permute-start | bytes 983048 | tf_op jit(solution)/shard_map/ppermute | solution.py:22
  59.4 9.3 %collective-permute-start.24 = (bf16[5,64,512]{2,1,0:T(8,128)(2,1)S(1)}, bf16[5,64,512]{2,1,0:T(8,128)(2,1)S(1)}, u32[]{:S(2)}, u32[]{:S(2)}) collective-permute-start(bf16[5,64,512]{2,1,0:T(8,128)(2,1)S(1)} %shard_map.197.refs_2_), channel_id=1, source_target_pairs={{0,4},{4,0},{1,5},{5,1},{2,6},{6,2},{3,7},{7,3},{8,12},{12,8},{9,1... | collective-permute-start | bytes 983048 | tf_op jit(solution)/shard_map/ppermute | solution.py:22
  59.5 10.8 %collective-permute-start.25 = (bf16[5,64,512]{2,1,0:T(8,128)(2,1)S(1)}, bf16[5,64,512]{2,1,0:T(8,128)(2,1)S(1)}, u32[]{:S(2)}, u32[]{:S(2)}) collective-permute-start(bf16[5,64,512]{2,1,0:T(8,128)(2,1)S(1)} %collective-permute-done.21.refs_3_), channel_id=1, source_target_pairs={{0,4},{4,0},{1,5},{5,1},{2,6},{6,2},{3,7},{7,3},{8,12},{12,8},{9,1... | collective-permute-start | bytes 983048 | tf_op jit(solution)/shard_map/ppermute | solution.py:22
  59.9 13.4 %collective-permute-start.26 = (bf16[5,64,512]{2,1,0:T(8,128)(2,1)S(1)}, bf16[5,64,512]{2,1,0:T(8,128)(2,1)S(1)}, u32[]{:S(2)}, u32[]{:S(2)}) collective-permute-start(bf16[5,64,512]{2,1,0:T(8,128)(2,1)S(1)} %collective-permute-done.22.refs_4_), channel_id=1, source_target_pairs={{0,4},{4,0},{1,5},{5,1},{2,6},{6,2},{3,7},{7,3},{8,12},{12,8},{9,1... | collective-permute-start | bytes 983048 | tf_op jit(solution)/shard_map/ppermute | solution.py:22
  60.4 13.7 %collective-permute-start.28 = (bf16[3,64,512]{2,1,0:T(8,128)(2,1)}, bf16[3,64,512]{2,1,0:T(8,128)(2,1)}, u32[]{:S(2)}, u32[]{:S(2)}) collective-permute-start(bf16[3,64,512]{2,1,0:T(8,128)(2,1)} %shard_map.198.refs_10_), channel_id=1, source_target_pairs={{0,8},{8,16},{16,24},{24,0},{1,9},{9,17},{17,25},{25,1},{2,10},{10... | collective-permute-start | bytes 589832 | tf_op jit(solution)/shard_map/ppermute | solution.py:22
  68.0 8.8 %collective-permute-start.29 = (bf16[3,64,512]{2,1,0:T(8,128)(2,1)}, bf16[3,64,512]{2,1,0:T(8,128)(2,1)}, u32[]{:S(2)}, u32[]{:S(2)}) collective-permute-start(bf16[3,64,512]{2,1,0:T(8,128)(2,1)} %shard_map.198.refs_10_), channel_id=1, source_target_pairs={{0,16},{8,24},{16,0},{24,8},{1,17},{9,25},{17,1},{25,9},{2,18},{10... | collective-permute-start | bytes 589832 | tf_op jit(solution)/shard_map/ppermute | solution.py:22
  69.4 20.1 %collective-permute-start.18 = (bf16[48,2064]{1,0:T(8,128)(2,1)S(1)}, bf16[48,2064]{1,0:T(8,128)(2,1)S(1)}, u32[]{:S(2)}, u32[]{:S(2)}) collective-permute-start(bf16[48,2064]{1,0:T(8,128)(2,1)S(1)} %get-tuple-element.26), channel_id=1, source_target_pairs={{0,24},{8,0},{16,8},{24,16},{1,25},{9,1},{17,9},{25,17},{2,26},{10... | collective-permute-start | bytes 594440 | tf_op jit(solution)/shard_map/ppermute | solution.py:22
  71.0 18.4 %collective-permute-start.19 = (bf16[48,2064]{1,0:T(8,128)(2,1)S(1)}, bf16[48,2064]{1,0:T(8,128)(2,1)S(1)}, u32[]{:S(2)}, u32[]{:S(2)}) collective-permute-start(bf16[48,2064]{1,0:T(8,128)(2,1)S(1)} %get-tuple-element.25), channel_id=1, source_target_pairs={{0,16},{8,24},{16,0},{24,8},{1,17},{9,25},{17,1},{25,9},{2,18},{10... | collective-permute-start | bytes 594440 | tf_op jit(solution)/shard_map/ppermute | solution.py:22
  74.1 16.6 %collective-permute-start.20 = (bf16[48,2064]{1,0:T(8,128)(2,1)S(1)}, bf16[48,2064]{1,0:T(8,128)(2,1)S(1)}, u32[]{:S(2)}, u32[]{:S(2)}) collective-permute-start(bf16[48,2064]{1,0:T(8,128)(2,1)S(1)} %get-tuple-element.24), channel_id=1, source_target_pairs={{0,8},{8,16},{16,24},{24,0},{1,9},{9,17},{17,25},{25,1},{2,10},{10... | collective-permute-start | bytes 594440 | tf_op jit(solution)/shard_map/ppermute | solution.py:22
  74.1 13.9 %collective-permute-start.30 = (bf16[3,64,512]{2,1,0:T(8,128)(2,1)}, bf16[3,64,512]{2,1,0:T(8,128)(2,1)}, u32[]{:S(2)}, u32[]{:S(2)}) collective-permute-start(bf16[3,64,512]{2,1,0:T(8,128)(2,1)} %shard_map.198.refs_10_), channel_id=1, source_target_pairs={{0,24},{8,0},{16,8},{24,16},{1,25},{9,1},{17,9},{25,17},{2,26},{10... | collective-permute-start | bytes 589832 | tf_op jit(solution)/shard_map/ppermute | solution.py:22
  76.8 22.4 %collective-permute-start.27 = (bf16[5,64,512]{2,1,0:T(8,128)(2,1)}, bf16[5,64,512]{2,1,0:T(8,128)(2,1)S(1)}, u32[]{:S(2)}, u32[]{:S(2)}) collective-permute-start(bf16[5,64,512]{2,1,0:T(8,128)(2,1)} %collective-permute-done.23.refs_5_), channel_id=1, source_target_pairs={{0,4},{4,0},{1,5},{5,1},{2,6},{6,2},{3,7},{7,3},{8,12},{12,8},{9,1... | collective-permute-start | bytes 983048 | tf_op jit(solution)/shard_map/ppermute | solution.py:22
  87.9 11.3 %collective-permute-start.31 = (bf16[3,64,512]{2,1,0:T(8,128)(2,1)}, bf16[3,64,512]{2,1,0:T(8,128)(2,1)}, u32[]{:S(2)}, u32[]{:S(2)}) collective-permute-start(bf16[3,64,512]{2,1,0:T(8,128)(2,1)} %shard_map.198.refs_10_), channel_id=1, source_target_pairs={{0,4},{4,0},{1,5},{5,1},{2,6},{6,2},{3,7},{7,3},{8,12},{12,8},{9,1... | collective-permute-start | bytes 589832 | tf_op jit(solution)/shard_map/ppermute | solution.py:22
  89.5 9.8 %collective-permute-start.32 = (bf16[3,64,512]{2,1,0:T(8,128)(2,1)}, bf16[3,64,512]{2,1,0:T(8,128)(2,1)}, u32[]{:S(2)}, u32[]{:S(2)}) collective-permute-start(bf16[3,64,512]{2,1,0:T(8,128)(2,1)} %collective-permute-done.28.refs_11_), channel_id=1, source_target_pairs={{0,4},{4,0},{1,5},{5,1},{2,6},{6,2},{3,7},{7,3},{8,12},{12,8},{9,1... | collective-permute-start | bytes 589832 | tf_op jit(solution)/shard_map/ppermute | solution.py:22
  90.2 9.1 %collective-permute-start.33 = (bf16[3,64,512]{2,1,0:T(8,128)(2,1)}, bf16[3,64,512]{2,1,0:T(8,128)(2,1)}, u32[]{:S(2)}, u32[]{:S(2)}) collective-permute-start(bf16[3,64,512]{2,1,0:T(8,128)(2,1)} %collective-permute-done.29.refs_12_), channel_id=1, source_target_pairs={{0,4},{4,0},{1,5},{5,1},{2,6},{6,2},{3,7},{7,3},{8,12},{12,8},{9,1... | collective-permute-start | bytes 589832 | tf_op jit(solution)/shard_map/ppermute | solution.py:22
  91.4 7.9 %collective-permute-start.34 = (bf16[3,64,512]{2,1,0:T(8,128)(2,1)}, bf16[3,64,512]{2,1,0:T(8,128)(2,1)}, u32[]{:S(2)}, u32[]{:S(2)}) collective-permute-start(bf16[3,64,512]{2,1,0:T(8,128)(2,1)} %collective-permute-done.30.refs_13_), channel_id=1, source_target_pairs={{0,4},{4,0},{1,5},{5,1},{2,6},{6,2},{3,7},{7,3},{8,12},{12,8},{9,1... | collective-permute-start | bytes 589832 | tf_op jit(solution)/shard_map/ppermute | solution.py:22
  (36 other events, 382.7 us)
